TPU v7x, 32 devices: a whole 2x2x4 slice. The times are simulated.
32 devices in a mesh: sp: 16 (over z, y, x), dp: 2 (over core).
Axes of the slice: x: 2, y: 2, z: 4, core: 2. Of those that a mesh axis runs over, the one named last changes fastest.
Arguments:
- queries: bfloat16 [2, 2048, 3072], P('dp', 'sp'), may hold values from -20 to 20
- kv_latent: bfloat16 [2, 2048, 256], P('dp', 'sp'), may hold values from -60 to 60
- rope_key: bfloat16 [2, 2048, 32], P('dp', 'sp'), may hold values from -20 to 20
- latent_norm_gain: float32 [256], replicated, may hold values from 0.1 to 1.9
- key_up_weight: bfloat16 [256, 2048], replicated, may hold values from -0.375 to 0.375
- value_up_weight: bfloat16 [256, 2048], replicated, may hold values from -0.375 to 0.375
- out_proj: bfloat16 [2048, 2048], replicated, may hold values from -0.125 to 0.125
- residual: bfloat16 [2, 2048, 2048], P('dp', 'sp'), may hold values from -0.59765625 to 0.59765625
- ffn_gain: float32 [2048], replicated, may hold values from 0.1 to 1.9
- routes: int32 [2, 2048, 2], P('dp', 'sp'), may hold values from 0 to 31, all different within a row; in each aligned block of 128 rows (0 to 127, 128 to 255, ..., all dimensions but the last counted through in order) at most 16 rows name the same one
- route_weights: float32 [2, 2048, 2], P('dp', 'sp'), may hold values from 0.1 to 1
- expert_gate: bfloat16 [32, 2048, 1024], P(('sp', 'dp')), may hold values from -1.3258252 to 1.3258252
- expert_up: bfloat16 [32, 2048, 1024], P(('sp', 'dp')), may hold values from -1.3258252 to 1.3258252
- expert_down: bfloat16 [32, 1024, 2048], P(('sp', 'dp')), may hold values from -0.1875 to 0.1875
Outputs:
- normed_rows: bfloat16 [2, 2048, 2048], P('dp', 'sp')
- layer_out: bfloat16 [2, 2048, 2048], P('dp', 'sp')
Inputs may be any that keep to these rules, and one draw needn't show every extreme that they name: `routes`: each token names 2 different experts. Among the tokens of one device no expert is named more than 16 times, and in some devices' tokens an expert is named exactly 16 times.
All inputs are finite; a program needn't handle non-finite values.
Results may differ from a plain program's by a relative error of at most 0.012.
The roundings to bfloat16 on the way count: a program that leaves them out, or rounds other values in their place, can miss the bound.
Values may be sent and summed in bfloat16 or wider, within the bound.
A program may use at most 128 MiB of HBM per device.

v0:
```python
import functools

import jax
import jax.numpy as jnp
import numpy as np
from jax import lax
from jax.experimental import pallas as pl
from jax.experimental.pallas import tpu as pltpu
from jax.sharding import PartitionSpec as P

PLAIN = 64
ROT = 32
QK = PLAIN + ROT
VALUE = 64
GRID_W = 64
GROUP = 4

eps_norm = 1e-06
rope_base = 10000.0
clamp_limit = 7.0
glu_alpha = 1.702

F32 = jnp.float32
BF16 = jnp.bfloat16
MESH_ID = pl.DeviceIdType.MESH
VMEM_LIMIT = 60 * 1024 * 1024


def params(**kw):
    return pltpu.CompilerParams(vmem_limit_bytes=VMEM_LIMIT, **kw)


def turn_tables(positions):
    pair = np.arange(ROT) // 2
    quarter = ROT // 4
    frequency = rope_base ** (-(2.0 * jnp.arange(quarter, dtype=F32)) / (ROT // 2))
    grid_row = (positions // GRID_W).astype(F32)
    grid_col = (positions % GRID_W).astype(F32)
    base = jnp.where(jnp.asarray(pair < quarter)[None, :], grid_row[:, None], grid_col[:, None])
    angle = base * frequency[pair % quarter][None, :]
    cosine, sine = lax.optimization_barrier((jnp.cos(angle), jnp.sin(angle)))
    even = jnp.asarray(np.arange(ROT) % 2 == 0)[None, :]
    return cosine, jnp.where(even, -sine, 0.0), jnp.where(even, 0.0, sine)


def group_table(table, plain):
    rest = jnp.full((table.shape[0], PLAIN), plain, F32)
    return jnp.concatenate([rest, table] * GROUP, axis=1)


def gather_kernel(axis_size, src, dst, send_sem, recv_sem, own_sem):
    sp = lax.axis_index("sp")
    dp = lax.axis_index("dp")
    barrier = pltpu.get_barrier_semaphore()

    def greet(k, _):
        pl.semaphore_signal(
            barrier, inc=1, device_id=(lax.rem(sp + k, axis_size), dp), device_id_type=MESH_ID
        )
        return 0

    lax.fori_loop(1, axis_size, greet, 0)
    own = pltpu.make_async_copy(src, dst.at[sp], own_sem)
    own.start()
    pl.semaphore_wait(barrier, axis_size - 1)

    half = axis_size // 2
    first = sp // half * half
    partner = lax.rem(sp + half, axis_size)

    def copy(block, other, slot):
        return pltpu.make_async_remote_copy(
            src_ref=src if block is None else dst.at[block],
            dst_ref=dst.at[sp if block is None else block],
            send_sem=send_sem.at[slot],
            recv_sem=recv_sem.at[slot],
            device_id=(other, dp),
            device_id_type=MESH_ID,
        )

    def near(k):
        return first + lax.rem(sp - first + k, half)

    def across():
        return copy(None, partner, 0)

    def own_near(k):
        return copy(None, near(k), k)

    def far_near(k):
        return copy(partner, near(k), half + k)

    def start_own(k, _):
        own_near(k).start()
        return 0

    def start_far(k, _):
        far_near(k).start()
        return 0

    def wait(k, _):
        own_near(k).wait()
        far_near(k).wait()
        return 0

    across().start()
    lax.fori_loop(1, half, start_own, 0)
    across().wait()
    lax.fori_loop(1, half, start_far, 0)
    lax.fori_loop(1, half, wait, 0)
    own.wait()


def gather_rows(rows, axis_size):
    return pl.pallas_call(
        functools.partial(gather_kernel, axis_size),
        out_shape=jax.ShapeDtypeStruct((axis_size,) + rows.shape, rows.dtype),
        in_specs=[pl.BlockSpec(memory_space=pl.ANY)],
        out_specs=pl.BlockSpec(memory_space=pl.ANY),
        scratch_shapes=[
            pltpu.SemaphoreType.DMA((axis_size,)),
            pltpu.SemaphoreType.DMA((axis_size,)),
            pltpu.SemaphoreType.DMA,
        ],
        compiler_params=params(collective_id=0, has_side_effects=True),
        name="latent_gather",
    )(rows)


def exchange_kernel(count, dp_size, src, dst, send_sem, recv_sem, own_sem):
    me = lax.axis_index("sp") * dp_size + lax.axis_index("dp")
    barrier = pltpu.get_barrier_semaphore()

    def place(k):
        return lax.rem(me + k, count)

    def device(k):
        other = place(k)
        return (other // dp_size, lax.rem(other, dp_size))

    def greet(k, _):
        pl.semaphore_signal(barrier, inc=1, device_id=device(k), device_id_type=MESH_ID)
        return 0

    lax.fori_loop(1, count, greet, 0)
    own = pltpu.make_async_copy(src.at[me], dst.at[me], own_sem)
    own.start()
    pl.semaphore_wait(barrier, count - 1)

    def copy(k):
        return pltpu.make_async_remote_copy(
            src_ref=src.at[place(k)],
            dst_ref=dst.at[me],
            send_sem=send_sem.at[k],
            recv_sem=recv_sem.at[k],
            device_id=device(k),
            device_id_type=MESH_ID,
        )

    def start(k, _):
        copy(k).start()
        return 0

    def wait(k, _):
        copy(k).wait()
        return 0

    lax.fori_loop(1, count, start, 0)
    lax.fori_loop(1, count, wait, 0)
    own.wait()


def exchange(blocks, dp_size, collective_id):
    count = blocks.shape[0]
    if blocks.shape[1] % 16:
        return lax.all_to_all(blocks, ("sp", "dp"), split_axis=0, concat_axis=0, tiled=True)
    return pl.pallas_call(
        functools.partial(exchange_kernel, count, dp_size),
        out_shape=jax.ShapeDtypeStruct(blocks.shape, blocks.dtype),
        in_specs=[pl.BlockSpec(memory_space=pl.ANY)],
        out_specs=pl.BlockSpec(memory_space=pl.ANY),
        scratch_shapes=[
            pltpu.SemaphoreType.DMA((count,)),
            pltpu.SemaphoreType.DMA((count,)),
            pltpu.SemaphoreType.DMA,
        ],
        compiler_params=params(collective_id=collective_id, has_side_effects=True),
        name="expert_exchange",
    )(blocks)


def dot(a, b, dims=((1,), (0,))):
    return lax.dot_general(a, b, (dims, ((), ())), preferred_element_type=F32)


def lane_fold(x, op):
    parts = [x[:, i : i + 128] for i in range(0, x.shape[1], 128)]
    return functools.reduce(op, parts)


def attention_kernel(
    experts, capacity, chunk,
    q_ref, cos_ref, next_ref, prev_ref, kup_ref, vup_ref, oproj_ref, keys_ref,
    res_ref, gain_ref, routes_ref,
    normed_ref, mixed_ref, out_ref, pick_ref,
    kt, lat, acc, qs, scores,
):
    step = pl.program_id(0)
    blocks, _, width = keys_ref.shape
    tok = q_ref.shape[0]
    half = ROT // 2
    rows = GROUP * tok

    @pl.when(step == 0)
    def _():
        acc[...] = jnp.zeros_like(acc)

        def fill(s, _):
            at = pl.ds(pl.multiple_of(s * tok, tok), tok)
            block = keys_ref[s]
            lat[at, :] = block[:tok]
            kt[:width, at] = block[:tok].T
            kt[width : width + half, at] = block[tok:, :tok]
            kt[width + half :, at] = block[tok:, tok : 2 * tok]
            return 0

        lax.fori_loop(0, blocks, fill, 0)

    x = q_ref[...].astype(F32)
    lanes = x.shape[1]
    turned = (
        x * cos_ref[...]
        + pltpu.roll(x, lanes - 1, 1) * next_ref[...]
        + pltpu.roll(x, 1, 1) * prev_ref[...]
    ) * (QK ** (-0.5))
    for i in range(GROUP):
        at = slice(i * tok, (i + 1) * tok)
        plain = turned[:, i * QK : i * QK + PLAIN].astype(BF16)
        absorbed = dot(plain, kup_ref[:, i * PLAIN : (i + 1) * PLAIN], ((1,), (1,)))
        qs[at, :width] = absorbed.astype(BF16)
        qs[at, width:] = turned[:, i * QK + PLAIN : (i + 1) * QK].astype(BF16)

    chunks = lat.shape[0] // chunk
    unroll = chunks <= 4

    def chunk_at(c):
        return pl.ds(c * chunk if unroll else pl.multiple_of(c * chunk, chunk), chunk)

    def loop(body, carry):
        if not unroll:
            return lax.fori_loop(0, chunks, body, carry)
        for c in range(chunks):
            carry = body(c, carry)
        return carry

    def score(c, top):
        s = dot(qs[...], kt[:, chunk_at(c)])
        scores[:, chunk_at(c)] = s
        return jnp.maximum(top, lane_fold(s, jnp.maximum))

    top = loop(score, jnp.full((rows, 128), -jnp.inf, F32))
    highest = jnp.max(top, axis=1, keepdims=True)

    def weigh(c, carry):
        total, context = carry
        w = jnp.exp(scores[:, chunk_at(c)] - highest)
        total = total + lane_fold(w, jnp.add)
        context = context + dot(w.astype(BF16), lat[chunk_at(c), :])
        return total, context

    total, context = loop(weigh, (jnp.zeros((rows, 128), F32), jnp.zeros((rows, width), F32)))
    context = (context / jnp.sum(total, axis=1, keepdims=True)).astype(BF16)
    heads = [
        dot(context[i * tok : (i + 1) * tok], vup_ref[:, i * VALUE : (i + 1) * VALUE])
        for i in range(GROUP)
    ]
    acc[...] += dot(jnp.concatenate(heads, axis=1).astype(BF16), oproj_ref[...])

    @pl.when(step == pl.num_programs(0) - 1)
    def _():
        mixed = res_ref[...].astype(F32) + acc[...]
        mixed_ref[...] = mixed
        square = jnp.mean(mixed * mixed, axis=1, keepdims=True)
        normed = (mixed * lax.rsqrt(square + eps_norm) * gain_ref[...]).astype(BF16)
        normed_ref[...] = normed
        slots = experts * capacity
        expert_lane = lax.broadcasted_iota(jnp.int32, (tok, experts), 1)
        slot_lane = lax.broadcasted_iota(jnp.int32, (tok, slots), 1)
        earlier = (
            lax.broadcasted_iota(jnp.int32, (tok, tok), 1)
            < lax.broadcasted_iota(jnp.int32, (tok, tok), 0)
        ).astype(F32)
        routes = routes_ref[...]
        taken = jnp.zeros((1, experts), F32)
        picks = []
        for k in range(routes.shape[1]):
            expert = routes[:, k : k + 1]
            named = (expert_lane == expert).astype(F32)
            before = dot(earlier.astype(BF16), named.astype(BF16)) + taken
            rank = jnp.sum(before * named, axis=1, keepdims=True)
            slot = expert * capacity + rank.astype(jnp.int32)
            pick = (slot_lane == slot).astype(F32)
            pick_ref[k * tok : (k + 1) * tok, :] = pick.astype(BF16)
            picks.append(pick)
            taken = taken + jnp.sum(named, axis=0, keepdims=True)
        spread = functools.reduce(jnp.add, picks).T.astype(BF16)
        out_ref[...] = dot(spread, normed).astype(BF16)


def attention(q, tables, kup, vup, oproj, keys, res, gain, routes, experts, capacity):
    tok, d = res.shape
    width = kup.shape[0]
    blocks = keys.shape[0]
    length = blocks * tok
    chunk = min(512, length)
    groups = q.shape[1] // (GROUP * QK)
    slots = experts * capacity
    picks = routes.shape[1] * tok

    def whole(*shape):
        return pl.BlockSpec(shape, lambda g: (0,) * len(shape))

    table = whole(tok, GROUP * QK)
    return pl.pallas_call(
        functools.partial(attention_kernel, experts, capacity, chunk),
        grid=(groups,),
        in_specs=[
            pl.BlockSpec((tok, GROUP * QK), lambda g: (0, g)),
            table, table, table,
            pl.BlockSpec((width, GROUP * PLAIN), lambda g: (0, g)),
            pl.BlockSpec((width, GROUP * VALUE), lambda g: (0, g)),
            pl.BlockSpec((GROUP * VALUE, d), lambda g: (g, 0)),
            whole(*keys.shape),
            whole(tok, d),
            whole(1, d),
            whole(*routes.shape),
        ],
        out_specs=[whole(tok, d), whole(tok, d), whole(slots, d), whole(picks, slots)],
        out_shape=[
            jax.ShapeDtypeStruct((tok, d), BF16),
            jax.ShapeDtypeStruct((tok, d), F32),
            jax.ShapeDtypeStruct((slots, d), BF16),
            jax.ShapeDtypeStruct((picks, slots), BF16),
        ],
        scratch_shapes=[
            pltpu.VMEM((width + ROT, length), BF16),
            pltpu.VMEM((length, width), BF16),
            pltpu.VMEM((tok, d), F32),
            pltpu.VMEM((GROUP * tok, width + ROT), BF16),
            pltpu.VMEM((GROUP * tok, length), F32),
        ],
        compiler_params=params(dimension_semantics=("arbitrary",)),
        name="attention",
    )(q, *tables, kup, vup, oproj, keys, res, gain, routes)


def expert_kernel(x_ref, gate_ref, up_ref, down_ref, out_ref, acc):
    step = pl.program_id(0)
    x = x_ref[...]
    gate = jnp.minimum(dot(x, gate_ref[...]), clamp_limit)
    up = jnp.clip(dot(x, up_ref[...]), -clamp_limit, clamp_limit)
    hidden = (gate * jax.nn.sigmoid(glu_alpha * gate) * (up + 1.0)).astype(BF16)
    part = dot(hidden, down_ref[...])

    @pl.when(step == 0)
    def _():
        acc[...] = part

    @pl.when(step > 0)
    def _():
        acc[...] += part

    @pl.when(step == pl.num_programs(0) - 1)
    def _():
        out_ref[...] = acc[...].astype(BF16)


def expert_rows(x, gate_w, up_w, down_w):
    rows, d = x.shape
    ff = gate_w.shape[1]
    tile = 256
    return pl.pallas_call(
        expert_kernel,
        grid=(ff // tile,),
        in_specs=[
            pl.BlockSpec((rows, d), lambda f: (0, 0)),
            pl.BlockSpec((d, tile), lambda f: (0, f)),
            pl.BlockSpec((d, tile), lambda f: (0, f)),
            pl.BlockSpec((tile, d), lambda f: (f, 0)),
        ],
        out_specs=pl.BlockSpec((rows, d), lambda f: (0, 0)),
        out_shape=jax.ShapeDtypeStruct((rows, d), BF16),
        scratch_shapes=[pltpu.VMEM((rows, d), F32)],
        compiler_params=params(dimension_semantics=("arbitrary",)),
        name="experts",
    )(x, gate_w, up_w, down_w)


def combine_kernel(pick_ref, back_ref, weight_ref, mixed_ref, out_ref):
    tok = mixed_ref.shape[0]
    rows = dot(pick_ref[...], back_ref[...])
    total = mixed_ref[...]
    routed = None
    for k in range(weight_ref.shape[1]):
        term = rows[k * tok : (k + 1) * tok] * weight_ref[:, k : k + 1]
        routed = term if routed is None else routed + term
    out_ref[...] = (total + routed).astype(BF16)


def combine(pick, back, weight, mixed):
    tok, d = mixed.shape
    slots = back.shape[0]
    tile = 512
    return pl.pallas_call(
        combine_kernel,
        grid=(d // tile,),
        in_specs=[
            pl.BlockSpec(pick.shape, lambda j: (0, 0)),
            pl.BlockSpec((slots, tile), lambda j: (0, j)),
            pl.BlockSpec(weight.shape, lambda j: (0, 0)),
            pl.BlockSpec((tok, tile), lambda j: (0, j)),
        ],
        out_specs=pl.BlockSpec((tok, tile), lambda j: (0, j)),
        out_shape=jax.ShapeDtypeStruct((tok, d), BF16),
        compiler_params=params(dimension_semantics=("arbitrary",)),
        name="combine",
    )(pick, back, weight, mixed)


def local(
    queries,
    kv_latent,
    rope_key,
    latent_norm_gain,
    key_up_weight,
    value_up_weight,
    out_proj,
    residual,
    ffn_gain,
    routes,
    route_weights,
    expert_gate,
    expert_up,
    expert_down,
):
    tok = queries.shape[1]
    d = residual.shape[2]
    topk = routes.shape[2]
    sp_size = lax.axis_size("sp")
    dp_size = lax.axis_size("dp")
    experts = sp_size * dp_size
    capacity = max(2, 2 * tok * topk // experts)
    positions = lax.axis_index("sp") * tok + jnp.arange(tok, dtype=jnp.int32)
    tables = turn_tables(positions)
    latent_float = kv_latent[0].astype(F32)
    latent = (
        latent_float
        * lax.rsqrt(jnp.mean(latent_float * latent_float, axis=-1, keepdims=True) + eps_norm)
        * latent_norm_gain
    ).astype(BF16)
    key = rope_key[0].astype(F32)
    cos_t, next_t, prev_t = tables
    key_turned = (
        key * cos_t + jnp.roll(key, -1, axis=1) * next_t + jnp.roll(key, 1, axis=1) * prev_t
    ).astype(BF16)
    key_columns = key_turned.T
    packed_keys = jnp.concatenate([key_columns[: ROT // 2], key_columns[ROT // 2 :]], axis=1)
    keys = gather_rows(jnp.concatenate([latent, packed_keys], axis=0), sp_size)
    wide_tables = [group_table(t, p) for t, p in zip(tables, (1.0, 0.0, 0.0))]
    normed, mixed, outgoing, pick = attention(
        queries[0], wide_tables, key_up_weight, value_up_weight, out_proj, keys,
        residual[0], ffn_gain[None], routes[0], experts, capacity,
    )
    blocks = outgoing.reshape(experts, capacity, d)
    slot_rows = exchange(blocks, dp_size, 1).reshape(experts * capacity, d)
    expert_out = expert_rows(slot_rows, expert_gate[0], expert_up[0], expert_down[0])
    back = exchange(expert_out.reshape(blocks.shape), dp_size, 2)
    layer_out = combine(pick, back.reshape(experts * capacity, d), route_weights[0], mixed)
    return (normed[None], layer_out[None])


def solution(mesh):
    in_specs = (
        P("dp", "sp", None),
        P("dp", "sp", None),
        P("dp", "sp", None),
        P(),
        P(),
        P(),
        P(),
        P("dp", "sp", None),
        P(),
        P("dp", "sp", None),
        P("dp", "sp", None),
        P(("sp", "dp"), None, None),
        P(("sp", "dp"), None, None),
        P(("sp", "dp"), None, None),
    )
    out_specs = (P("dp", "sp", None), P("dp", "sp", None))
    return jax.shard_map(local, mesh=mesh, in_specs=in_specs, out_specs=out_specs, check_vma=False)
```

profile of v0, /device:TPU:15, one launch (start us, length us, event | category | flops | bytes accessed | tf_op | source)
XLA Modules:
  0.0 195.0 jit_solution(11172552294769904980)
XLA Ops:
  0.7 0.7 pad_clamp_fusion
  1.3 0.7 gather_fusion
  2.0 1.0 fusion.6
  3.0 0.8 copy.39
  3.9 0.1 fusion.11
  3.9 0.1 fusion.12
  4.0 0.8 fusion.8
  4.8 0.1 fusion.13
  4.9 0.1 copy.40
  5.0 0.1 copy.41
  5.1 0.1 fusion
  5.2 0.1 fusion.2
  5.3 0.6 maximum_maximum_fusion.src
  6.0 20.2 %latent_gather.1.keys_ref = bf16[16,144,256]{2,1,0:T(8,128)(2,1)} custom-call(bf16[144,256]{1,0:T(8,128)(2,1)} %maximum_maximum_fusion.src), custom_call_target="tpu_custom_call" | custom-call | tf_op jit(solution)/shard_map/latent_gather/pallas_call | solution.py:115
  26.2 0.8 concatenate.25.prev_ref
  27.0 0.9 concatenate.24.next_ref
  27.9 0.8 concatenate.23.cos_ref
  28.7 0.7 copy.42
  29.5 37.3 %attention.1 = (bf16[128,2048]{1,0:T(8,128)(2,1)}, f32[128,2048]{1,0:T(8,128)}, bf16[512,2048]{1,0:T(8,128)(2,1)}, bf16[256,512]{1,0:T(8,128)(2,1)}) custom-call(bf16[128,3072]{1,0:T(8,128)(2,1)} %bitcast.32, f32[128,384]{1,0:T(8,128)} %concatenate.23.cos_ref, f32[128,384]{1,0:T(8,128)} %concatenate.24.next_ref, f32[128,384]{1,0:T(8,128)} %concatenate.25.prev_ref, ...), custom_call_target="tpu_custom_call" | custom-call | tf_op jit(solution)/shard_map/attention/pallas_call | solution.py:324
  66.8 56.1 %expert_exchange.2 = bf16[32,16,2048]{2,1,0:T(8,128)(2,1)} custom-call(bf16[32,16,2048]{2,1,0:T(8,128)(2,1)} %bitcast.31), custom_call_target="tpu_custom_call" | custom-call | tf_op jit(solution)/shard_map/expert_exchange/pallas_call | solution.py:177
  122.9 13.3 %experts.1 = bf16[512,2048]{1,0:T(8,128)(2,1)} custom-call(bf16[512,2048]{1,0:T(8,128)(2,1)} %bitcast.26, bf16[2048,1024]{1,0:T(8,128)(2,1)} %bitcast.28, bf16[2048,1024]{1,0:T(8,128)(2,1)} %bitcast.29, bf16[1024,2048]{1,0:T(8,128)(2,1)} %bitcast.30), custom_call_target="tpu_custom_call" | custom-call | tf_op jit(solution)/shard_map/experts/pallas_call | solution.py:382
  136.2 53.8 %expert_exchange.3 = bf16[32,16,2048]{2,1,0:T(8,128)(2,1)} custom-call(bf16[32,16,2048]{2,1,0:T(8,128)(2,1)} %bitcast.27), custom_call_target="tpu_custom_call" | custom-call | tf_op jit(solution)/shard_map/expert_exchange/pallas_call | solution.py:177
  190.0 0.7 copy.43
  190.7 4.3 %combine.1 = bf16[128,2048]{1,0:T(8,128)(2,1)} custom-call(bf16[256,512]{1,0:T(8,128)(2,1)} %get-tuple-element.11.pick_ref, bf16[512,2048]{1,0:T(8,128)(2,1)} %bitcast.25, f32[128,2]{1,0:T(8,128)} %bitcast.36, f32[128,2048]{1,0:T(8,128)} %get-tuple-element.13.mixed_ref), custom_call_target="tpu_custom_call" | custom-call | tf_op jit(solution)/shard_map/combine/pallas_call | solution.py:414
  (14 shorter events, 0.1 us)
Async XLA Ops:
  0.6 4.4 %copy-start = (bf16[1,128,256]{2,1,0:T(8,128)(2,1)S(1)}, bf16[1,128,256]{2,1,0:T(8,128)(2,1)}, u32[]{:S(2)}) copy-start(bf16[1,128,256]{2,1,0:T(8,128)(2,1)} %param.19) | copy-start | bytes 196612
  0.6 4.6 %copy-start.1 = (f32[256]{0:T(256)S(1)}, f32[256]{0:T(256)}, u32[]{:S(2)}) copy-start(f32[256]{0:T(256)} %param.21) | copy-start | bytes 3076
  4.8 23.9 %copy-start.2 = (s32[1,128,2]{1,2,0:T(2,128)S(1)}, s32[1,128,2]{1,2,0:T(2,128)}, u32[]{:S(2)}) copy-start(s32[1,128,2]{1,2,0:T(2,128)} %param.27) | copy-start | bytes 3076
  136.2 53.8 %copy-start.3 = (f32[1,128,2]{1,2,0:T(2,128)S(1)}, f32[1,128,2]{1,2,0:T(2,128)}, u32[]{:S(2)}) copy-start(f32[1,128,2]{1,2,0:T(2,128)} %param.28) | copy-start | bytes 3076
where the time goes:
time: 195 us
  Pallas kernels  185 us (95%)
  local copies, waits for them, and re-layouts  5.94 us (3%)
  other arithmetic  3.33 us (2%)
    pallas_call x2, Pallas kernels, exchange(): pl.pallas_call(functools.partial(exchange_kernel, count, dp_size), out_sh...  110 us
    pallas_call x1, Pallas kernels, attention(): pl.pallas_call(functools.partial(attention_kernel, experts, capacity, chu...  37.3 us
    pallas_call x1, Pallas kernels, gather_rows(): pl.pallas_call(functools.partial(gather_kernel, axis_size), out_shape=jax...  20.2 us
    pallas_call x1, Pallas kernels, expert_rows(): pl.pallas_call(expert_kernel, grid=(ff // tile,), in_specs=[pl.BlockSpec(...  13.3 us
    pallas_call x1, Pallas kernels, combine(): pl.pallas_call(combine_kernel, grid=(d // tile,), in_specs=[pl.BlockSpec(...  4.31 us

commit v1 on v0

v1 whole, which is shorter than its diff:
```python
import functools

import jax
import jax.numpy as jnp
import numpy as np
from jax import lax
from jax.experimental import pallas as pl
from jax.experimental.pallas import tpu as pltpu
from jax.sharding import PartitionSpec as P

PLAIN = 64
ROT = 32
QK = PLAIN + ROT
VALUE = 64
GRID_W = 64
GROUP = 4

eps_norm = 1e-06
rope_base = 10000.0
clamp_limit = 7.0
glu_alpha = 1.702

F32 = jnp.float32
BF16 = jnp.bfloat16
MESH_ID = pl.DeviceIdType.MESH
VMEM_LIMIT = 60 * 1024 * 1024


def params(**kw):
    return pltpu.CompilerParams(vmem_limit_bytes=VMEM_LIMIT, **kw)


PLANE = 4
CHUNK = 512


def turn_tables(length):
    pair = np.arange(ROT) // 2
    quarter = ROT // 4
    frequency = (rope_base ** (-(2.0 * np.arange(quarter)) / (ROT // 2))).astype(np.float32)
    even = np.arange(ROT) % 2 == 0

    def part(places, mine, plain):
        angle = places.astype(np.float32)[:, None] * frequency[pair % quarter][None, :]
        cosine, sine = np.cos(angle.astype(np.float64)), np.sin(angle.astype(np.float64))
        tables = [cosine, np.where(even, -sine, 0.0), np.where(even, 0.0, sine)]
        wide = []
        for table, rest in zip(tables, plain):
            head = np.concatenate(
                [np.full((len(places), PLAIN), rest), np.where(mine, table, 0.0)], axis=1
            )
            wide += [head] * GROUP
        return np.concatenate(wide, axis=1).astype(np.float32)

    rows = part(np.arange(-(-length // GRID_W)), pair < quarter, (0.0, 0.0, 0.0))
    cols = part(np.arange(GRID_W), pair >= quarter, (1.0, 0.0, 0.0))
    return rows, cols


def exchange_kernel(count, dp_size, src, dst, send_sem, recv_sem, own_sem):
    me = lax.axis_index("sp") * dp_size + lax.axis_index("dp")
    barrier = pltpu.get_barrier_semaphore()

    def place(k):
        return lax.rem(me + k, count)

    def device(k):
        other = place(k)
        return (other // dp_size, lax.rem(other, dp_size))

    def greet(k, _):
        pl.semaphore_signal(barrier, inc=1, device_id=device(k), device_id_type=MESH_ID)
        return 0

    lax.fori_loop(1, count, greet, 0)
    own = pltpu.make_async_copy(src.at[me], dst.at[me], own_sem)
    own.start()
    pl.semaphore_wait(barrier, count - 1)

    def copy(k):
        return pltpu.make_async_remote_copy(
            src_ref=src.at[place(k)],
            dst_ref=dst.at[me],
            send_sem=send_sem.at[k],
            recv_sem=recv_sem.at[k],
            device_id=device(k),
            device_id_type=MESH_ID,
        )

    def start(k, _):
        copy(k).start()
        return 0

    def wait(k, _):
        copy(k).wait()
        return 0

    lax.fori_loop(1, count, start, 0)
    lax.fori_loop(1, count, wait, 0)
    own.wait()


def exchange(blocks, dp_size, collective_id):
    count = blocks.shape[0]
    if blocks.shape[1] % 16:
        return lax.all_to_all(blocks, ("sp", "dp"), split_axis=0, concat_axis=0, tiled=True)
    return pl.pallas_call(
        functools.partial(exchange_kernel, count, dp_size),
        out_shape=jax.ShapeDtypeStruct(blocks.shape, blocks.dtype),
        in_specs=[pl.BlockSpec(memory_space=pl.ANY)],
        out_specs=pl.BlockSpec(memory_space=pl.ANY),
        scratch_shapes=[
            pltpu.SemaphoreType.DMA((count,)),
            pltpu.SemaphoreType.DMA((count,)),
            pltpu.SemaphoreType.DMA,
        ],
        compiler_params=params(collective_id=collective_id, has_side_effects=True),
        name="expert_exchange",
    )(blocks)


def dot(a, b, dims=((1,), (0,))):
    return lax.dot_general(a, b, (dims, ((), ())), preferred_element_type=F32)


def lane_fold(x, op):
    parts = [x[:, i : i + 128] for i in range(0, x.shape[1], 128)]
    return functools.reduce(op, parts)


def attention_kernel(
    sp_size, experts, capacity,
    q_hbm, kup_hbm, vup_hbm, oproj_hbm, res_hbm,
    latent_ref, key_ref, lgain_ref, rows_ref, cols_ref, gain_ref, routes_ref,
    normed_ref, mixed_ref, out_ref, pick_ref,
    q, kup, vup, oproj, res, blocks, kt, lat, tab, qs, acc,
    scores_a, scores_b, top_a, top_b, load_sem, send_sem, recv_sem,
):
    sp = lax.axis_index("sp")
    dp = lax.axis_index("dp")
    tok = latent_ref.shape[0]
    width = latent_ref.shape[1]
    line = sp_size // PLANE
    z, p = sp // PLANE, lax.rem(sp, PLANE)
    x_near = z * PLANE + p + 1 - 2 * lax.rem(p, 2)
    y_near = z * PLANE + lax.rem(p + 2, PLANE)
    p_x, p_y = lax.rem(x_near, PLANE), lax.rem(y_near, PLANE)
    half_rot = ROT // 2

    def column(k):
        return lax.rem(z + k, line) * PLANE + p

    barrier = pltpu.get_barrier_semaphore()

    def greet(other):
        pl.semaphore_signal(barrier, inc=1, device_id=(other, dp), device_id_type=MESH_ID)

    def greet_line(k, _):
        greet(column(k))
        return 0

    lax.fori_loop(1, line, greet_line, 0)
    greet(x_near)
    greet(y_near)

    loads = [
        pltpu.make_async_copy(src, dst, load_sem.at[i])
        for i, (src, dst) in enumerate(
            [(q_hbm, q), (kup_hbm, kup), (vup_hbm, vup), (res_hbm, res), (oproj_hbm, oproj)]
        )
    ]
    for load in loads:
        load.start()

    grid_rows = tok // GRID_W
    lanes = GROUP * QK
    for s in range(grid_rows):
        wide = cols_ref[...] + rows_ref[pl.ds(sp * grid_rows + s, 1), :]
        for i in range(3):
            tab[i, s * GRID_W : (s + 1) * GRID_W, :] = wide[:, i * lanes : (i + 1) * lanes]

    def turn(x, width):
        return (
            x * tab[0, :, :width]
            + pltpu.roll(x, width - 1, 1) * tab[1, :, :width]
            + pltpu.roll(x, 1, 1) * tab[2, :, :width]
        )

    latent_float = latent_ref[...].astype(F32)
    square = jnp.mean(latent_float * latent_float, axis=1, keepdims=True)
    latent = latent_float * lax.rsqrt(square + eps_norm) * lgain_ref[...]
    blocks[sp, :tok, :] = latent.astype(BF16)
    key = key_ref[...].astype(F32)
    key = jnp.concatenate(
        [jnp.zeros((tok, PLAIN), F32), key, jnp.zeros((tok, 128 - QK), F32)], axis=1
    )
    key_columns = turn(key, 128).T.astype(BF16)
    blocks[sp, tok:, :tok] = key_columns[PLAIN : PLAIN + half_rot]
    blocks[sp, tok:, tok:] = key_columns[PLAIN + half_rot : QK]

    def copy(block, other, slot):
        return pltpu.make_async_remote_copy(
            src_ref=blocks.at[block],
            dst_ref=blocks.at[block],
            send_sem=send_sem.at[slot],
            recv_sem=recv_sem.at[block],
            device_id=(other, dp),
            device_id_type=MESH_ID,
        )

    def to_line(k):
        return copy(sp, column(k), k)

    def to_x(k):
        return copy(column(k), x_near, line + k)

    def to_y(k):
        return copy(column(k), y_near, 2 * line + k)

    def relay_y(k):
        return copy(k * PLANE + p_x, y_near, 3 * line + k)

    def relay_x(k):
        return copy(k * PLANE + p_y, x_near, 4 * line + k)

    def arrive(block):
        copy(block, sp, 0).wait_recv()

    def fill(block):
        at = pl.ds(pl.multiple_of(block * tok, tok), tok)
        lat[at, :] = blocks[block, :tok, :]
        kt[:width, at] = blocks[block, :tok, :].T
        kt[width : width + half_rot, at] = blocks[block, tok:, :tok]
        kt[width + half_rot :, at] = blocks[block, tok:, tok:]

    pl.semaphore_wait(barrier, line + 1)

    def start_line(k, _):
        to_line(k).start()
        return 0

    lax.fori_loop(1, line, start_line, 0)
    to_x(0).start()
    to_y(0).start()

    half = tok // 2
    rows = 2 * GROUP * half
    sets = q.shape[1] // lanes
    loads[0].wait()
    loads[1].wait()

    def prepare(j, _):
        x = q[:, pl.ds(pl.multiple_of(j * lanes, 128), lanes)].astype(F32)
        turned = turn(x, lanes) * (QK ** (-0.5))
        up = kup[:, pl.ds(pl.multiple_of(j * GROUP * PLAIN, 128), GROUP * PLAIN)]
        for i in range(GROUP):
            plain = turned[:, i * QK : i * QK + PLAIN].astype(BF16)
            absorbed = dot(plain, up[:, i * PLAIN : (i + 1) * PLAIN], ((1,), (1,))).astype(BF16)
            rotary = turned[:, i * QK + PLAIN : (i + 1) * QK].astype(BF16)
            at = slice(i * half, (i + 1) * half)
            for h in range(2):
                mine = slice(h * half, (h + 1) * half)
                qs[h * sets + j, at, :width] = absorbed[mine]
                qs[h * sets + j, at, width:] = rotary[mine]
        return 0

    early = sets // 4
    lax.fori_loop(0, early, prepare, 0)

    def pass_on(k, _):
        back = line - k
        block = column(back)
        arrive(block)
        to_x(back).start()
        to_y(back).start()
        return 0

    lax.fori_loop(1, line, pass_on, 0)
    lax.fori_loop(early, sets, prepare, 0)

    def fill_column(k, _):
        fill(k * PLANE + p)
        return 0

    lax.fori_loop(0, line, fill_column, 0)

    def relay(k, _):
        other = lax.rem(z + k, line)
        from_x, from_y = other * PLANE + p_x, other * PLANE + p_y
        arrive(from_x)

        @pl.when(lax.rem(other, 2) == 0)
        def _():
            relay_y(other).start()

        arrive(from_y)

        @pl.when(lax.rem(other, 2) == 1)
        def _():
            relay_x(other).start()

        fill(from_x)
        fill(from_y)
        return 0

    lax.fori_loop(0, line, relay, 0)

    def last(k, _):
        other = lax.rem(z + k, line)
        block = other * PLANE + (PLANE - 1 - p)
        arrive(block)
        fill(block)
        return 0

    lax.fori_loop(0, line, last, 0)

    length = lat.shape[0]
    chunk = min(CHUNK, length)
    groups = sets // 2
    for load in loads[2:]:
        load.wait()

    def score(g, scores, top):
        mine = qs[pl.ds(2 * g, 2)].reshape(rows, width + ROT)
        best = None
        for c in range(0, length, chunk):
            s = dot(mine, kt[:, c : c + chunk])
            scores[:, c : c + chunk] = s
            part = lane_fold(s, jnp.maximum)
            best = part if best is None else jnp.maximum(best, part)
        top[...] = best

    def weigh(g, scores, top):
        highest = jnp.max(top[...], axis=1, keepdims=True)
        total = context = None
        for c in range(0, length, chunk):
            w = jnp.exp(scores[:, c : c + chunk] - highest)
            part = lane_fold(w, jnp.add)
            seen = dot(w.astype(BF16), lat[c : c + chunk, :])
            total = part if total is None else total + part
            context = seen if context is None else context + seen
        context = (context / jnp.sum(total, axis=1, keepdims=True)).astype(BF16)
        spread = 2 * GROUP * VALUE
        at = pl.ds(pl.multiple_of(lax.rem(g, groups) * spread, spread), spread)
        up = vup[:, at]
        heads = [
            dot(context[i * half : (i + 1) * half], up[:, i * VALUE : (i + 1) * VALUE])
            for i in range(2 * GROUP)
        ]
        acc[...] += dot(jnp.concatenate(heads, axis=1).astype(BF16), oproj[at, :])

    def settle(h):
        at = pl.ds(pl.multiple_of(h * half, half), half)
        mixed = res[at, :].astype(F32) + acc[...]
        mixed_ref[at, :] = mixed
        mean = jnp.mean(mixed * mixed, axis=1, keepdims=True)
        normed_ref[at, :] = (mixed * lax.rsqrt(mean + eps_norm) * gain_ref[...]).astype(BF16)
        acc[...] = jnp.zeros_like(acc)

    acc[...] = jnp.zeros_like(acc)
    score(0, scores_a, top_a)

    def two(i, _):
        g = 2 * i
        weigh(g, scores_a, top_a)
        score(g + 1, scores_b, top_b)
        weigh(g + 1, scores_b, top_b)
        score(g + 2, scores_a, top_a)

        @pl.when(g + 2 == groups)
        def _():
            settle(0)

        return 0

    lax.fori_loop(0, groups - 1, two, 0)
    weigh(2 * groups - 2, scores_a, top_a)
    score(2 * groups - 1, scores_b, top_b)
    weigh(2 * groups - 1, scores_b, top_b)
    settle(1)

    slots = experts * capacity
    expert_lane = lax.broadcasted_iota(jnp.int32, (tok, experts), 1)
    slot_lane = lax.broadcasted_iota(jnp.int32, (tok, slots), 1)
    earlier = (
        lax.broadcasted_iota(jnp.int32, (tok, tok), 1)
        < lax.broadcasted_iota(jnp.int32, (tok, tok), 0)
    ).astype(BF16)
    routes = routes_ref[...]
    taken = jnp.zeros((1, experts), F32)
    picks = []
    for k in range(routes.shape[1]):
        expert = routes[:, k : k + 1]
        named = (expert_lane == expert).astype(F32)
        before = dot(earlier, named.astype(BF16)) + taken
        rank = jnp.sum(before * named, axis=1, keepdims=True)
        slot = expert * capacity + rank.astype(jnp.int32)
        pick = (slot_lane == slot).astype(F32)
        pick_ref[k * tok : (k + 1) * tok, :] = pick.astype(BF16)
        picks.append(pick)
        taken = taken + jnp.sum(named, axis=0, keepdims=True)
    spread = functools.reduce(jnp.add, picks).T.astype(BF16)
    out_ref[...] = dot(spread, normed_ref[...]).astype(BF16)

    def sent(k, _):
        to_x(k).wait_send()
        to_y(k).wait_send()

        @pl.when(k > 0)
        def _():
            to_line(k).wait_send()

        @pl.when(lax.rem(k, 2) == 0)
        def _():
            relay_y(k).wait_send()

        @pl.when(lax.rem(k, 2) == 1)
        def _():
            relay_x(k).wait_send()

        return 0

    lax.fori_loop(0, line, sent, 0)


def attention(q, latent, key, lgain, kup, vup, oproj, res, gain, routes, sp_size, experts, capacity):
    tok, d = res.shape
    width = latent.shape[1]
    length = sp_size * tok
    slots = experts * capacity
    picks = routes.shape[1] * tok
    lanes = GROUP * QK
    sets = q.shape[1] // lanes
    rows = GROUP * tok
    row_table, col_table = turn_tables(length)
    far = pl.BlockSpec(memory_space=pl.ANY)
    near = pl.BlockSpec(memory_space=pltpu.VMEM)
    return pl.pallas_call(
        functools.partial(attention_kernel, sp_size, experts, capacity),
        in_specs=[far] * 5 + [near] * 7,
        out_specs=[near] * 4,
        out_shape=[
            jax.ShapeDtypeStruct((tok, d), BF16),
            jax.ShapeDtypeStruct((tok, d), F32),
            jax.ShapeDtypeStruct((slots, d), BF16),
            jax.ShapeDtypeStruct((picks, slots), BF16),
        ],
        scratch_shapes=[
            pltpu.VMEM(q.shape, BF16),
            pltpu.VMEM(kup.shape, BF16),
            pltpu.VMEM(vup.shape, BF16),
            pltpu.VMEM(oproj.shape, BF16),
            pltpu.VMEM(res.shape, BF16),
            pltpu.VMEM((sp_size, tok + ROT // 2, width), BF16),
            pltpu.VMEM((width + ROT, length), BF16),
            pltpu.VMEM((length, width), BF16),
            pltpu.VMEM((3, tok, lanes), F32),
            pltpu.VMEM((2 * sets, rows // 2, width + ROT), BF16),
            pltpu.VMEM((tok // 2, d), F32),
            pltpu.VMEM((rows, length), F32),
            pltpu.VMEM((rows, length), F32),
            pltpu.VMEM((rows, 128), F32),
            pltpu.VMEM((rows, 128), F32),
            pltpu.SemaphoreType.DMA((5,)),
            pltpu.SemaphoreType.DMA((5 * sp_size // PLANE,)),
            pltpu.SemaphoreType.DMA((sp_size,)),
        ],
        compiler_params=params(collective_id=0, has_side_effects=True),
        name="attention",
    )(q, kup, vup, oproj, res, latent, key, lgain, row_table, col_table, gain, routes)


def expert_kernel(x_ref, gate_ref, up_ref, down_ref, out_ref, acc):
    step = pl.program_id(0)
    x = x_ref[...]
    gate = jnp.minimum(dot(x, gate_ref[...]), clamp_limit)
    up = jnp.clip(dot(x, up_ref[...]), -clamp_limit, clamp_limit)
    hidden = (gate * jax.nn.sigmoid(glu_alpha * gate) * (up + 1.0)).astype(BF16)
    part = dot(hidden, down_ref[...])

    @pl.when(step == 0)
    def _():
        acc[...] = part

    @pl.when(step > 0)
    def _():
        acc[...] += part

    @pl.when(step == pl.num_programs(0) - 1)
    def _():
        out_ref[...] = acc[...].astype(BF16)


def expert_rows(x, gate_w, up_w, down_w):
    rows, d = x.shape
    ff = gate_w.shape[1]
    tile = 256
    return pl.pallas_call(
        expert_kernel,
        grid=(ff // tile,),
        in_specs=[
            pl.BlockSpec((rows, d), lambda f: (0, 0)),
            pl.BlockSpec((d, tile), lambda f: (0, f)),
            pl.BlockSpec((d, tile), lambda f: (0, f)),
            pl.BlockSpec((tile, d), lambda f: (f, 0)),
        ],
        out_specs=pl.BlockSpec((rows, d), lambda f: (0, 0)),
        out_shape=jax.ShapeDtypeStruct((rows, d), BF16),
        scratch_shapes=[pltpu.VMEM((rows, d), F32)],
        compiler_params=params(dimension_semantics=("arbitrary",)),
        name="experts",
    )(x, gate_w, up_w, down_w)


def combine_kernel(pick_ref, back_ref, weight_ref, mixed_ref, out_ref):
    tok = mixed_ref.shape[0]
    rows = dot(pick_ref[...], back_ref[...])
    total = mixed_ref[...]
    routed = None
    for k in range(weight_ref.shape[1]):
        term = rows[k * tok : (k + 1) * tok] * weight_ref[:, k : k + 1]
        routed = term if routed is None else routed + term
    out_ref[...] = (total + routed).astype(BF16)


def combine(pick, back, weight, mixed):
    tok, d = mixed.shape
    slots = back.shape[0]
    tile = 512
    return pl.pallas_call(
        combine_kernel,
        grid=(d // tile,),
        in_specs=[
            pl.BlockSpec(pick.shape, lambda j: (0, 0)),
            pl.BlockSpec((slots, tile), lambda j: (0, j)),
            pl.BlockSpec(weight.shape, lambda j: (0, 0)),
            pl.BlockSpec((tok, tile), lambda j: (0, j)),
        ],
        out_specs=pl.BlockSpec((tok, tile), lambda j: (0, j)),
        out_shape=jax.ShapeDtypeStruct((tok, d), BF16),
        compiler_params=params(dimension_semantics=("arbitrary",)),
        name="combine",
    )(pick, back, weight, mixed)


def local(
    queries,
    kv_latent,
    rope_key,
    latent_norm_gain,
    key_up_weight,
    value_up_weight,
    out_proj,
    residual,
    ffn_gain,
    routes,
    route_weights,
    expert_gate,
    expert_up,
    expert_down,
):
    tok = queries.shape[1]
    d = residual.shape[2]
    topk = routes.shape[2]
    sp_size = lax.axis_size("sp")
    dp_size = lax.axis_size("dp")
    experts = sp_size * dp_size
    capacity = max(2, 2 * tok * topk // experts)
    normed, mixed, outgoing, pick = attention(
        queries[0], kv_latent[0], rope_key[0], latent_norm_gain[None], key_up_weight,
        value_up_weight, out_proj, residual[0], ffn_gain[None], routes[0],
        sp_size, experts, capacity,
    )
    blocks = outgoing.reshape(experts, capacity, d)
    slot_rows = exchange(blocks, dp_size, 1).reshape(experts * capacity, d)
    expert_out = expert_rows(slot_rows, expert_gate[0], expert_up[0], expert_down[0])
    back = exchange(expert_out.reshape(blocks.shape), dp_size, 2)
    layer_out = combine(pick, back.reshape(experts * capacity, d), route_weights[0], mixed)
    return (normed[None], layer_out[None])


def solution(mesh):
    in_specs = (
        P("dp", "sp", None),
        P("dp", "sp", None),
        P("dp", "sp", None),
        P(),
        P(),
        P(),
        P(),
        P("dp", "sp", None),
        P(),
        P("dp", "sp", None),
        P("dp", "sp", None),
        P(("sp", "dp"), None, None),
        P(("sp", "dp"), None, None),
        P(("sp", "dp"), None, None),
    )
    out_specs = (P("dp", "sp", None), P("dp", "sp", None))
    return jax.shard_map(local, mesh=mesh, in_specs=in_specs, out_specs=out_specs, check_vma=False)
```

time: 195 us -> 187 us (0.959)
  other arithmetic: 3.33 us -> 0 us
  Pallas kernels: 185 us -> 182 us
    pallas_call x2 -> x1, Pallas kernels: 57.5 us -> 50.3 us  [attention(): pl.pallas_call(functools.partial(attention_kernel, sp_size, experts, capa...]
    pallas_call x2, Pallas kernels: 110 us -> 114 us  [exchange(): pl.pallas_call(functools.partial(exchange_kernel, count, dp_size), out_sh...]
    concatenate x3 -> x0, local copies, waits for them, and re-layouts: 2.55 us -> none  [group_table(): return jnp.concatenate([rest, table] * GROUP, axis=1)]
    unnamed x11 -> x8, local copies, waits for them, and re-layouts: 2.3 us -> 4.37 us
where the time goes in v1:
time: 187 us
  Pallas kernels  182 us (97%)
  local copies, waits for them, and re-layouts  4.37 us (2%)
    pallas_call x2, Pallas kernels, exchange(): pl.pallas_call(functools.partial(exchange_kernel, count, dp_size), out_sh...  114 us
    pallas_call x1, Pallas kernels, attention(): pl.pallas_call(functools.partial(attention_kernel, sp_size, experts, capa...  50.3 us
    pallas_call x1, Pallas kernels, expert_rows(): pl.pallas_call(expert_kernel, grid=(ff // tile,), in_specs=[pl.BlockSpec(...  13.3 us
    unnamed x8, local copies, waits for them, and re-layouts  4.37 us
    pallas_call x1, Pallas kernels, combine(): pl.pallas_call(combine_kernel, grid=(d // tile,), in_specs=[pl.BlockSpec(...  4.31 us

profile of v1, /device:TPU:15, one launch (start us, length us, event | category | flops | bytes accessed | tf_op | source)
XLA Modules:
  0.0 186.8 jit_solution(11013757281540139158)
XLA Ops:
  0.6 1.4 copy.19
  2.0 1.4 copy.18
  3.5 50.3 %attention.1 = (bf16[128,2048]{1,0:T(8,128)(2,1)}, f32[128,2048]{1,0:T(8,128)}, bf16[512,2048]{1,0:T(8,128)(2,1)}, bf16[256,512]{1,0:T(8,128)(2,1)}) custom-call(bf16[128,3072]{1,0:T(8,128)(2,1)} %bitcast.24, bf16[256,2048]{1,0:T(8,128)(2,1)} %kup_hbm.1, bf16[256,2048]{1,0:T(8,128)(2,1)} %vup_hbm.1, bf16[2048,2048]{1,0:T(8,128)(2,1)} %oproj_hbm.1, ...), custom_call_target="tpu_custom_call" | custom-call | tf_op jit(solution)/shard_map/attention/pallas_call | solution.py:438
  53.8 58.7 %expert_exchange.2 = bf16[32,16,2048]{2,1,0:T(8,128)(2,1)} custom-call(bf16[32,16,2048]{2,1,0:T(8,128)(2,1)} %bitcast.23), custom_call_target="tpu_custom_call" | custom-call | tf_op jit(solution)/shard_map/expert_exchange/pallas_call | solution.py:107
  112.5 13.3 %experts.1 = bf16[512,2048]{1,0:T(8,128)(2,1)} custom-call(bf16[512,2048]{1,0:T(8,128)(2,1)} %bitcast.18, bf16[2048,1024]{1,0:T(8,128)(2,1)} %bitcast.20, bf16[2048,1024]{1,0:T(8,128)(2,1)} %bitcast.21, bf16[1024,2048]{1,0:T(8,128)(2,1)} %bitcast.22), custom_call_target="tpu_custom_call" | custom-call | tf_op jit(solution)/shard_map/experts/pallas_call | solution.py:498
  125.8 0.0 copy-start.1
  125.8 0.0 copy-start
  125.8 55.1 %expert_exchange.3 = bf16[32,16,2048]{2,1,0:T(8,128)(2,1)} custom-call(bf16[32,16,2048]{2,1,0:T(8,128)(2,1)} %bitcast.19), custom_call_target="tpu_custom_call" | custom-call | tf_op jit(solution)/shard_map/expert_exchange/pallas_call | solution.py:107
  180.9 0.0 copy-done.1
  180.9 0.7 copy.20
  181.7 4.3 %combine.1 = bf16[128,2048]{1,0:T(8,128)(2,1)} custom-call(bf16[256,512]{1,0:T(8,128)(2,1)} %get-tuple-element.7.pick_ref, bf16[512,2048]{1,0:T(8,128)(2,1)} %bitcast.17, f32[128,2]{1,0:T(8,128)} %bitcast.29, f32[128,2048]{1,0:T(8,128)} %get-tuple-element.9.mixed_ref), custom_call_target="tpu_custom_call" | custom-call | tf_op jit(solution)/shard_map/combine/pallas_call | solution.py:530
  186.0 0.0 copy-done
  186.0 0.8 copy.22
Async XLA Ops:
  125.8 55.2 %copy-start.1 = (f32[1,128,2]{1,2,0:T(2,128)S(1)}, f32[1,128,2]{1,2,0:T(2,128)}, u32[]{:S(2)}) copy-start(f32[1,128,2]{1,2,0:T(2,128)} %param.26) | copy-start | bytes 3076
  125.8 60.2 %copy-start = (bf16[128,2048]{1,0:T(8,128)(2,1)S(1)}, bf16[128,2048]{1,0:T(8,128)(2,1)}, u32[]{:S(2)}) copy-start(bf16[128,2048]{1,0:T(8,128)(2,1)} %get-tuple-element.6) | copy-start | bytes 1572868

commit v2 on v1

v2 whole, which is shorter than its diff:
```python
import functools
import types

import jax
import jax.numpy as jnp
import numpy as np
from jax import lax
from jax.experimental import pallas as pl
from jax.experimental.pallas import tpu as pltpu
from jax.sharding import PartitionSpec as P

PLAIN = 64
ROT = 32
QK = PLAIN + ROT
VALUE = 64
GRID_W = 64
GROUP = 4

eps_norm = 1e-06
rope_base = 10000.0
clamp_limit = 7.0
glu_alpha = 1.702

F32 = jnp.float32
BF16 = jnp.bfloat16
MESH_ID = pl.DeviceIdType.MESH
VMEM_LIMIT = 60 * 1024 * 1024
LAYER_VMEM = 63 * 1024 * 1024 + 900 * 1024


def params(**kw):
    return pltpu.CompilerParams(**{'vmem_limit_bytes': VMEM_LIMIT, **kw})


PLANE = 4
CHUNK = 512


def turn_tables(length):
    pair = np.arange(ROT) // 2
    quarter = ROT // 4
    frequency = (rope_base ** (-(2.0 * np.arange(quarter)) / (ROT // 2))).astype(np.float32)
    even = np.arange(ROT) % 2 == 0

    def part(places, mine, plain):
        angle = places.astype(np.float32)[:, None] * frequency[pair % quarter][None, :]
        cosine, sine = np.cos(angle.astype(np.float64)), np.sin(angle.astype(np.float64))
        tables = [cosine, np.where(even, -sine, 0.0), np.where(even, 0.0, sine)]
        wide = []
        for table, rest in zip(tables, plain):
            head = np.concatenate(
                [np.full((len(places), PLAIN), rest), np.where(mine, table, 0.0)], axis=1
            )
            wide += [head] * GROUP
        return np.concatenate(wide, axis=1).astype(np.float32)

    rows = part(np.arange(-(-length // GRID_W)), pair < quarter, (0.0, 0.0, 0.0))
    cols = part(np.arange(GRID_W), pair >= quarter, (1.0, 0.0, 0.0))
    return rows, cols


def exchange_kernel(count, dp_size, src, dst, send_sem, recv_sem, own_sem):
    me = lax.axis_index("sp") * dp_size + lax.axis_index("dp")
    barrier = pltpu.get_barrier_semaphore()

    def place(k):
        return lax.rem(me + k, count)

    def device(k):
        other = place(k)
        return (other // dp_size, lax.rem(other, dp_size))

    def greet(k, _):
        pl.semaphore_signal(barrier, inc=1, device_id=device(k), device_id_type=MESH_ID)
        return 0

    lax.fori_loop(1, count, greet, 0)
    own = pltpu.make_async_copy(src.at[me], dst.at[me], own_sem)
    own.start()
    pl.semaphore_wait(barrier, count - 1)

    def copy(k):
        return pltpu.make_async_remote_copy(
            src_ref=src.at[place(k)],
            dst_ref=dst.at[me],
            send_sem=send_sem.at[k],
            recv_sem=recv_sem.at[k],
            device_id=device(k),
            device_id_type=MESH_ID,
        )

    def start(k, _):
        copy(k).start()
        return 0

    def wait(k, _):
        copy(k).wait()
        return 0

    lax.fori_loop(1, count, start, 0)
    lax.fori_loop(1, count, wait, 0)
    own.wait()


def exchange(blocks, dp_size, collective_id):
    count = blocks.shape[0]
    if blocks.shape[1] % 16:
        return lax.all_to_all(blocks, ("sp", "dp"), split_axis=0, concat_axis=0, tiled=True)
    return pl.pallas_call(
        functools.partial(exchange_kernel, count, dp_size),
        out_shape=jax.ShapeDtypeStruct(blocks.shape, blocks.dtype),
        in_specs=[pl.BlockSpec(memory_space=pl.ANY)],
        out_specs=pl.BlockSpec(memory_space=pl.ANY),
        scratch_shapes=[
            pltpu.SemaphoreType.DMA((count,)),
            pltpu.SemaphoreType.DMA((count,)),
            pltpu.SemaphoreType.DMA,
        ],
        compiler_params=params(collective_id=collective_id, has_side_effects=True),
        name="expert_exchange",
    )(blocks)


def dot(a, b, dims=((1,), (0,))):
    return lax.dot_general(a, b, (dims, ((), ())), preferred_element_type=F32)


def lane_fold(x, op):
    parts = [x[:, i : i + 128] for i in range(0, x.shape[1], 128)]
    return functools.reduce(op, parts)


def layer_kernel(names, sizes, *refs):
    r = types.SimpleNamespace(**dict(zip(names, refs)))
    sp_size, dp_size, experts, capacity, fused = sizes
    sp = lax.axis_index("sp")
    dp = lax.axis_index("dp")
    tok, width = r.latent.shape
    d = r.res.shape[1]
    topk = r.routes.shape[0]
    length = sp_size * tok
    line = sp_size // PLANE
    z, p = sp // PLANE, lax.rem(sp, PLANE)
    x_near = z * PLANE + p + 1 - 2 * lax.rem(p, 2)
    y_near = z * PLANE + lax.rem(p + 2, PLANE)
    p_x, p_y = lax.rem(x_near, PLANE), lax.rem(y_near, PLANE)
    half_rot = ROT // 2
    half = tok // 2
    rows = 2 * GROUP * half
    lanes = GROUP * QK
    sets = r.q.shape[1] // lanes
    groups = sets // 2
    tile = min(512, d)
    me = sp * dp_size + dp

    def column(k):
        return lax.rem(z + k, line) * PLANE + p

    barrier = pltpu.get_barrier_semaphore()

    def greet(place, other_dp):
        pl.semaphore_signal(barrier, inc=1, device_id=(place, other_dp), device_id_type=MESH_ID)

    if fused:
        greeted = sp_size * dp_size - 1

        def greet_other(k, _):
            other = lax.rem(me + k, sp_size * dp_size)
            greet(other // dp_size, lax.rem(other, dp_size))
            return 0

        lax.fori_loop(1, greeted + 1, greet_other, 0)
    else:
        greeted = line + 1

        def greet_line(k, _):
            greet(column(k), dp)
            return 0

        lax.fori_loop(1, line, greet_line, 0)
        greet(x_near, dp)
        greet(y_near, dp)

    loaded = [
        "latent", "key", "lgain", "row_table", "col_table", "routes",
        "q", "kup", "vup", "res", "oproj", "gain",
    ]
    if fused:
        loaded += ["weights", "gate", "up", "down"]
    loads = {
        name: pltpu.make_async_copy(getattr(r, name + "_hbm"), getattr(r, name), r.load_sem.at[i])
        for i, name in enumerate(loaded)
    }
    for name in loaded:
        loads[name].start()
    for name in loaded[:6]:
        loads[name].wait()

    grid_rows = tok // GRID_W
    for s in range(grid_rows):
        wide = r.col_table[...] + r.row_table[pl.ds(sp * grid_rows + s, 1), :]
        for i in range(3):
            r.tab[i, s * GRID_W : (s + 1) * GRID_W, :] = wide[:, i * lanes : (i + 1) * lanes]

    def turn(x, wide):
        return (
            x * r.tab[0, :, :wide]
            + pltpu.roll(x, wide - 1, 1) * r.tab[1, :, :wide]
            + pltpu.roll(x, 1, 1) * r.tab[2, :, :wide]
        )

    blocks = r.blocks
    latent_float = r.latent[...].astype(F32)
    square = jnp.mean(latent_float * latent_float, axis=1, keepdims=True)
    latent = latent_float * lax.rsqrt(square + eps_norm) * r.lgain[...]
    blocks[sp, :tok, :] = latent.astype(BF16)
    key = r.key[...].astype(F32)
    key = jnp.concatenate(
        [jnp.zeros((tok, PLAIN), F32), key, jnp.zeros((tok, 128 - QK), F32)], axis=1
    )
    key_columns = turn(key, 128).T.astype(BF16)
    blocks[sp, tok:, :tok] = key_columns[PLAIN : PLAIN + half_rot]
    blocks[sp, tok:, tok:] = key_columns[PLAIN + half_rot : QK]
    if fused:
        r.line_routes[z] = jnp.concatenate(
            [r.routes[...], jnp.zeros((8 - topk, tok), jnp.int32)], axis=0
        )

    def remote(src, dst, send, recv, place, other_dp):
        return pltpu.make_async_remote_copy(
            src_ref=src,
            dst_ref=dst,
            send_sem=send,
            recv_sem=recv,
            device_id=(place, other_dp),
            device_id_type=MESH_ID,
        )

    def copy(block, other, slot):
        block = blocks.at[block], r.recv_sem.at[block]
        return remote(block[0], block[0], r.send_sem.at[slot], block[1], other, dp)

    def to_line(k):
        return copy(sp, column(k), k)

    def to_x(k):
        return copy(column(k), x_near, line + k)

    def to_y(k):
        return copy(column(k), y_near, 2 * line + k)

    def relay_y(k):
        return copy(k * PLANE + p_x, y_near, 3 * line + k)

    def relay_x(k):
        return copy(k * PLANE + p_y, x_near, 4 * line + k)

    def arrive(block):
        copy(block, sp, 0).wait_recv()

    def routes_to(k, back=False):
        place = lax.rem(z + line - k, line) if back else z
        ref = r.line_routes.at[place]
        return remote(
            ref, ref, r.route_send.at[k], r.route_recv.at[place], column(k), dp
        )

    def fill(block):
        at = pl.ds(pl.multiple_of(block * tok, tok), tok)
        r.lat[at, :] = blocks[block, :tok, :]
        r.kt[:width, at] = blocks[block, :tok, :].T
        r.kt[width : width + half_rot, at] = blocks[block, tok:, :tok]
        r.kt[width + half_rot :, at] = blocks[block, tok:, tok:]

    loads["q"].wait()
    loads["kup"].wait()

    def prepare(j, _):
        x = r.q[:, pl.ds(pl.multiple_of(j * lanes, 128), lanes)].astype(F32)
        turned = turn(x, lanes) * (QK ** (-0.5))
        up = r.kup[:, pl.ds(pl.multiple_of(j * GROUP * PLAIN, 128), GROUP * PLAIN)]
        for i in range(GROUP):
            plain = turned[:, i * QK : i * QK + PLAIN].astype(BF16)
            absorbed = dot(plain, up[:, i * PLAIN : (i + 1) * PLAIN], ((1,), (1,))).astype(BF16)
            rotary = turned[:, i * QK + PLAIN : (i + 1) * QK].astype(BF16)
            at = slice(i * half, (i + 1) * half)
            for h in range(2):
                mine = slice(h * half, (h + 1) * half)
                r.qs[h * sets + j, at, :width] = absorbed[mine]
                r.qs[h * sets + j, at, width:] = rotary[mine]
        return 0

    pl.semaphore_wait(barrier, greeted)
    to_x(0).start()
    to_y(0).start()

    def start_line(k, _):
        to_line(k).start()
        if fused:
            routes_to(k).start()
        return 0

    lax.fori_loop(1, line, start_line, 0)
    early = sets // 4
    lax.fori_loop(0, early, prepare, 0)

    def pass_on(k, _):
        back = line - k
        arrive(column(back))
        to_x(back).start()
        to_y(back).start()
        return 0

    lax.fori_loop(1, line, pass_on, 0)
    lax.fori_loop(early, sets, prepare, 0)

    def fill_column(k, _):
        fill(k * PLANE + p)
        return 0

    lax.fori_loop(0, line, fill_column, 0)

    def relay(k, _):
        other = lax.rem(z + k, line)
        from_x, from_y = other * PLANE + p_x, other * PLANE + p_y
        arrive(from_x)

        @pl.when(lax.rem(other, 2) == 0)
        def _():
            relay_y(other).start()

        arrive(from_y)

        @pl.when(lax.rem(other, 2) == 1)
        def _():
            relay_x(other).start()

        fill(from_x)
        fill(from_y)
        return 0

    lax.fori_loop(0, line, relay, 0)

    def last(k, _):
        block = lax.rem(z + k, line) * PLANE + (PLANE - 1 - p)
        arrive(block)
        fill(block)
        return 0

    lax.fori_loop(0, line, last, 0)
    for name in ("vup", "res", "oproj", "gain"):
        loads[name].wait()

    chunk = min(CHUNK, length)
    buffers = [(r.scores_a, r.top_a), (r.scores_b, r.top_b)]

    def step(weighed, scored, slot):
        if scored is not None:
            mine = r.qs[pl.ds(2 * scored, 2)].reshape(rows, width + ROT)
            new_scores, new_top = buffers[slot]
        if weighed is not None:
            scores, top = buffers[1 - slot]
            highest = jnp.max(top[...], axis=1, keepdims=True)
        best = total = context = None
        for c in range(0, length, chunk):
            at = slice(c, c + chunk)
            if weighed is not None:
                w = jnp.exp(scores[:, at] - highest)
                part = lane_fold(w, jnp.add)
                seen = dot(w.astype(BF16), r.lat[at, :])
                total = part if total is None else total + part
                context = seen if context is None else context + seen
            if scored is not None:
                fresh = dot(mine, r.kt[:, at])
                new_scores[:, at] = fresh
                part = lane_fold(fresh, jnp.maximum)
                best = part if best is None else jnp.maximum(best, part)
        if scored is not None:
            new_top[...] = best
        if weighed is not None:
            context = context / jnp.sum(total, axis=1, keepdims=True)
            r.context[lax.rem(weighed, groups)] = context.astype(BF16)

    def settle(h):
        at = slice(h * half, (h + 1) * half)
        for j in range(groups):
            heads = [
                dot(
                    r.context[j, i * half : (i + 1) * half],
                    r.vup[:, (j * 2 * GROUP + i) * VALUE : (j * 2 * GROUP + i + 1) * VALUE],
                )
                for i in range(2 * GROUP)
            ]
            spread = 2 * GROUP * VALUE
            r.heads[:, j * spread : (j + 1) * spread] = jnp.concatenate(heads, axis=1).astype(BF16)
        square = jnp.zeros((half, 128), F32)
        for n in range(0, d, tile):
            part = r.res[at, n : n + tile].astype(F32) + dot(r.heads[...], r.oproj[:, n : n + tile])
            r.mixed[at, n : n + tile] = part
            square = square + lane_fold(part * part, jnp.add)
        scale = lax.rsqrt(jnp.sum(square, axis=1, keepdims=True) / d + eps_norm)
        normed = (r.mixed[at, :] * scale * r.gain[...]).astype(BF16)
        r.normed[at, :] = normed
        if fused:
            r.tokens[z, at, :] = normed

    def ship(block, h, up):
        ref = r.tokens.at[block, pl.ds(h * half, half), :]
        slot = ((2 if up else 0) + h) * line + block
        return remote(
            ref, ref, r.ship_send.at[slot], r.ship_recv.at[h * line + block],
            sp + PLANE if up else sp - PLANE, dp,
        )

    def ship_both(block, h, act):
        @pl.when((block <= z) & (z + 1 < line))
        def _():
            act(ship(block, h, True))

        @pl.when((block >= z) & (z > 0))
        def _():
            act(ship(block, h, False))

    def start(c):
        c.start()

    def forward(block, h):
        ship(block, h, True).wait_recv()
        ship_both(block, h, start)

    step(None, 0, 0)

    def two(i, _):
        g = 2 * i
        step(g, g + 1, 1)
        step(g + 1, g + 2, 0)

        @pl.when(g + 2 == groups)
        def _():
            settle(0)
            if fused:
                ship_both(z, 0, start)

        return 0

    lax.fori_loop(0, groups - 1, two, 0)
    step(2 * groups - 2, 2 * groups - 1, 1)
    if fused:

        @pl.when(z > 0)
        def _():
            forward(z - 1, 0)

        @pl.when(z + 1 < line)
        def _():
            forward(z + 1, 0)

    step(2 * groups - 1, None, 0)
    settle(1)

    expert_lane = lax.broadcasted_iota(jnp.int32, (tok, experts), 1)
    slot_lane = lax.broadcasted_iota(jnp.int32, (tok, experts * capacity), 1)
    place_a = lax.broadcasted_iota(jnp.int32, (tok, tok), 0)
    place_b = lax.broadcasted_iota(jnp.int32, (tok, tok), 1)

    def columns(part):
        rest = jnp.zeros((tok - topk, tok), F32)
        return jnp.concatenate([part.astype(F32), rest], axis=0).T

    def pick_rows():
        routes = columns(r.routes[...])
        earlier = (place_b < place_a).astype(BF16)
        taken = jnp.zeros((1, experts), F32)
        picks = []
        for k in range(topk):
            expert = routes[:, k : k + 1].astype(jnp.int32)
            named = (expert_lane == expert).astype(F32)
            before = dot(earlier, named.astype(BF16)) + taken
            rank = jnp.sum(before * named, axis=1, keepdims=True)
            slot = expert * capacity + rank.astype(jnp.int32)
            pick = (slot_lane == slot).astype(F32)
            r.pick[k * tok : (k + 1) * tok, :] = pick.astype(BF16)
            picks.append(pick)
            taken = taken + jnp.sum(named, axis=0, keepdims=True)
        return picks

    if fused:
        ship_both(z, 1, start)
        near = PLANE * dp_size
        mine = p * dp_size + dp
        local_row = lax.broadcasted_iota(jnp.int32, (near, tok), 0)
        slot_row = lax.broadcasted_iota(jnp.int32, (near * capacity, tok), 0)

        def wait_routes(k, _):
            routes_to(k, True).wait_recv()
            return 0

        lax.fori_loop(1, line, wait_routes, 0)

        def give(block, other):
            return remote(
                r.stage.at[block, other], r.inbox.at[block, mine],
                r.give_send.at[block * near + other], r.give_recv.at[block * near + mine],
                z * PLANE + other // dp_size, lax.rem(other, dp_size),
            )

        def given(block, other):
            return remote(
                r.stage.at[block, other], r.inbox.at[block, other],
                r.give_send.at[block * near + other], r.give_recv.at[block * near + other],
                z * PLANE + other // dp_size, lax.rem(other, dp_size),
            )

        def dispatch(block):
            later = (place_a < place_b).astype(F32)
            taken = jnp.zeros((near, 1), F32)
            spread = None
            for k in range(topk):
                route = r.line_routes[block, k : k + 1, :] - z * near
                named = (local_row == route).astype(F32)
                before = dot(named, later) + taken
                slot = local_row.astype(F32) * capacity + before + 1.0
                slot = jnp.sum(named * slot, axis=0, keepdims=True).astype(jnp.int32) - 1
                pick = slot_row == slot
                spread = pick if spread is None else spread | pick
                taken = taken + jnp.sum(named, axis=1, keepdims=True)
            spread = spread.astype(F32).astype(BF16)
            for n in range(0, d, tile):
                part = dot(spread, r.tokens[block, :, n : n + tile]).astype(BF16)
                r.stage[block, :, :, n : n + tile] = part.reshape(near, capacity, tile)
            r.inbox[block, mine] = r.stage[block, mine]

            def send(k, _):
                give(block, lax.rem(mine + k, near)).start()
                return 0

            lax.fori_loop(1, near, send, 0)

        def answer(block, other):
            return remote(
                r.outbox.at[block, other], r.back.at[me],
                r.back_send.at[block * near + other], r.back_recv.at[me],
                block * PLANE + other // dp_size, lax.rem(other, dp_size),
            )

        def answer_all(block, act):
            def one(other, _):
                @pl.when((block != z) | (other != mine))
                def _():
                    act(answer(block, other))

                return 0

            lax.fori_loop(0, near, one, 0)

        def expert(block):
            def wait(k, _):
                given(block, lax.rem(mine + k, near)).wait_recv()
                return 0

            lax.fori_loop(1, near, wait, 0)
            x = r.inbox[block].reshape(near * capacity, d)
            for n in range(0, r.gate.shape[1], 256):
                at = slice(n, n + 256)
                gate = jnp.minimum(dot(x, r.gate[:, at]), clamp_limit)
                up = jnp.clip(dot(x, r.up[:, at]), -clamp_limit, clamp_limit)
                hidden = gate * jax.nn.sigmoid(glu_alpha * gate) * (up + 1.0)
                r.hidden[:, at] = hidden.astype(BF16)
            for n in range(0, d, tile):
                part = dot(r.hidden[...], r.down[:, n : n + tile]).astype(BF16)
                r.outbox[block, :, :, n : n + tile] = part.reshape(near, capacity, tile)

            @pl.when(block == z)
            def _():
                r.back[me] = r.outbox[block, mine]

            answer_all(block, start)

        for name in ("weights", "gate", "up", "down"):
            loads[name].wait()

        def at_hop(t, act):
            block = z + jnp.where(lax.rem(t, 2) == 1, -((t + 1) // 2), t // 2)

            @pl.when((block >= 0) & (block < line))
            def _():
                act(block)

        lag = 2
        hops = 2 * line - 1

        def hop(t, _):
            def bring(block):
                @pl.when(t > 2)
                def _():
                    forward(block, 0)

                @pl.when(t > 0)
                def _():
                    forward(block, 1)

                dispatch(block)

            @pl.when(t < hops)
            def _():
                at_hop(t, bring)

            @pl.when(t >= lag)
            def _():
                at_hop(t - lag, expert)

            return 0

        lax.fori_loop(0, hops + lag, hop, 0)
        pick_rows()
        weights = columns(r.weights[...])

        def wait_back(k, _):
            other = lax.rem(me + k, experts)
            remote(
                r.outbox.at[0, 0], r.back.at[other], r.back_send.at[0], r.back_recv.at[other], sp, dp
            ).wait_recv()
            return 0

        lax.fori_loop(1, experts, wait_back, 0)
        for n in range(0, d, tile):
            back = r.back[:, :, n : n + tile].reshape(experts * capacity, tile)
            picked = dot(r.pick[...], back)
            routed = None
            for k in range(topk):
                term = picked[k * tok : (k + 1) * tok] * weights[:, k : k + 1]
                routed = term if routed is None else routed + term
            r.out[:, n : n + tile] = (r.mixed[:, n : n + tile] + routed).astype(BF16)

        def finish(block, _):
            def drain(c):
                c.wait_send()

            for h in range(2):
                ship_both(block, h, drain)
            answer_all(block, drain)

            def sent_all(k, _):
                give(block, lax.rem(mine + k, near)).wait_send()
                return 0

            lax.fori_loop(1, near, sent_all, 0)
            return 0

        lax.fori_loop(0, line, finish, 0)
    else:
        spread = functools.reduce(jnp.add, pick_rows()).T.astype(BF16)
        r.slots[...] = dot(spread, r.normed[...]).astype(BF16)

    def sent(k, _):
        to_x(k).wait_send()
        to_y(k).wait_send()

        @pl.when(k > 0)
        def _():
            to_line(k).wait_send()
            if fused:
                routes_to(k).wait_send()

        @pl.when(lax.rem(k, 2) == 0)
        def _():
            relay_y(k).wait_send()

        @pl.when(lax.rem(k, 2) == 1)
        def _():
            relay_x(k).wait_send()

        return 0

    lax.fori_loop(0, line, sent, 0)


def layer(operands, sp_size, dp_size, capacity, fused):
    tok, d = operands["res"].shape
    width = operands["latent"].shape[1]
    ff = operands["gate"].shape[1]
    topk = operands["routes"].shape[0]
    experts = sp_size * dp_size
    length = sp_size * tok
    line = sp_size // PLANE
    near = PLANE * dp_size
    slots = experts * capacity
    lanes = GROUP * QK
    sets = operands["q"].shape[1] // lanes
    rows = GROUP * tok
    if not fused:
        operands = {k: v for k, v in operands.items() if k not in ("weights", "gate", "up", "down")}
    inputs = list(operands)
    vmem, dma = pltpu.VMEM, pltpu.SemaphoreType.DMA
    scratch = {name: vmem(operands[name].shape, operands[name].dtype) for name in inputs}
    scratch.update(
        blocks=vmem((sp_size, tok + ROT // 2, width), BF16),
        kt=vmem((width + ROT, length), BF16),
        lat=vmem((length, width), BF16),
        tab=vmem((3, tok, lanes), F32),
        qs=vmem((2 * sets, rows // 2, width + ROT), BF16),
        context=vmem((sets // 2, rows, width), BF16),
        heads=vmem((tok // 2, sets * GROUP * VALUE), BF16),
        scores_a=vmem((rows, length), F32),
        scores_b=vmem((rows, length), F32),
        top_a=vmem((rows, 128), F32),
        top_b=vmem((rows, 128), F32),
        load_sem=dma((len(inputs),)),
        send_sem=dma((5 * line,)),
        recv_sem=dma((sp_size,)),
    )
    outputs = {"normed": jax.ShapeDtypeStruct((tok, d), BF16)}
    if fused:
        outputs["out"] = jax.ShapeDtypeStruct((tok, d), BF16)
        scratch.update(
            mixed=vmem((tok, d), F32),
            pick=vmem((topk * tok, slots), BF16),
            line_routes=vmem((line, 8, tok), jnp.int32),
            tokens=vmem((line, tok, d), BF16),
            stage=vmem((line, near, capacity, d), BF16),
            inbox=vmem((line, near, capacity, d), BF16),
            outbox=vmem((line, near, capacity, d), BF16),
            back=vmem((experts, capacity, d), BF16),
            hidden=vmem((near * capacity, ff), BF16),
            route_send=dma((line,)),
            route_recv=dma((line,)),
            ship_send=dma((4 * line,)),
            ship_recv=dma((2 * line,)),
            give_send=dma((line * near,)),
            give_recv=dma((line * near,)),
            back_send=dma((line * near,)),
            back_recv=dma((experts,)),
        )
    else:
        outputs["mixed"] = jax.ShapeDtypeStruct((tok, d), F32)
        outputs["slots"] = jax.ShapeDtypeStruct((slots, d), BF16)
        outputs["pick"] = jax.ShapeDtypeStruct((topk * tok, slots), BF16)
    names = [name + "_hbm" for name in inputs] + list(outputs) + list(scratch)
    return pl.pallas_call(
        functools.partial(layer_kernel, names, (sp_size, dp_size, experts, capacity, fused)),
        in_specs=[pl.BlockSpec(memory_space=pl.ANY)] * len(inputs),
        out_specs=[pl.BlockSpec(memory_space=pltpu.VMEM)] * len(outputs),
        out_shape=list(outputs.values()),
        scratch_shapes=list(scratch.values()),
        compiler_params=params(
            collective_id=0, has_side_effects=True, vmem_limit_bytes=LAYER_VMEM
        ),
        name="layer",
    )(*operands.values())


def expert_kernel(x_ref, gate_ref, up_ref, down_ref, out_ref, acc):
    step = pl.program_id(0)
    x = x_ref[...]
    gate = jnp.minimum(dot(x, gate_ref[...]), clamp_limit)
    up = jnp.clip(dot(x, up_ref[...]), -clamp_limit, clamp_limit)
    hidden = (gate * jax.nn.sigmoid(glu_alpha * gate) * (up + 1.0)).astype(BF16)
    part = dot(hidden, down_ref[...])

    @pl.when(step == 0)
    def _():
        acc[...] = part

    @pl.when(step > 0)
    def _():
        acc[...] += part

    @pl.when(step == pl.num_programs(0) - 1)
    def _():
        out_ref[...] = acc[...].astype(BF16)


def expert_rows(x, gate_w, up_w, down_w):
    rows, d = x.shape
    ff = gate_w.shape[1]
    tile = 256
    return pl.pallas_call(
        expert_kernel,
        grid=(ff // tile,),
        in_specs=[
            pl.BlockSpec((rows, d), lambda f: (0, 0)),
            pl.BlockSpec((d, tile), lambda f: (0, f)),
            pl.BlockSpec((d, tile), lambda f: (0, f)),
            pl.BlockSpec((tile, d), lambda f: (f, 0)),
        ],
        out_specs=pl.BlockSpec((rows, d), lambda f: (0, 0)),
        out_shape=jax.ShapeDtypeStruct((rows, d), BF16),
        scratch_shapes=[pltpu.VMEM((rows, d), F32)],
        compiler_params=params(dimension_semantics=("arbitrary",)),
        name="experts",
    )(x, gate_w, up_w, down_w)


def combine_kernel(pick_ref, back_ref, weight_ref, mixed_ref, out_ref):
    tok = mixed_ref.shape[0]
    rows = dot(pick_ref[...], back_ref[...])
    total = mixed_ref[...]
    routed = None
    for k in range(weight_ref.shape[1]):
        term = rows[k * tok : (k + 1) * tok] * weight_ref[:, k : k + 1]
        routed = term if routed is None else routed + term
    out_ref[...] = (total + routed).astype(BF16)


def combine(pick, back, weight, mixed):
    tok, d = mixed.shape
    slots = back.shape[0]
    tile = 512
    return pl.pallas_call(
        combine_kernel,
        grid=(d // tile,),
        in_specs=[
            pl.BlockSpec(pick.shape, lambda j: (0, 0)),
            pl.BlockSpec((slots, tile), lambda j: (0, j)),
            pl.BlockSpec(weight.shape, lambda j: (0, 0)),
            pl.BlockSpec((tok, tile), lambda j: (0, j)),
        ],
        out_specs=pl.BlockSpec((tok, tile), lambda j: (0, j)),
        out_shape=jax.ShapeDtypeStruct((tok, d), BF16),
        compiler_params=params(dimension_semantics=("arbitrary",)),
        name="combine",
    )(pick, back, weight, mixed)


def local(
    queries,
    kv_latent,
    rope_key,
    latent_norm_gain,
    key_up_weight,
    value_up_weight,
    out_proj,
    residual,
    ffn_gain,
    routes,
    route_weights,
    expert_gate,
    expert_up,
    expert_down,
):
    tok = queries.shape[1]
    d = residual.shape[2]
    topk = routes.shape[2]
    sp_size = lax.axis_size("sp")
    dp_size = lax.axis_size("dp")
    experts = sp_size * dp_size
    capacity = max(2, 2 * tok * topk // experts)
    row_table, col_table = turn_tables(sp_size * tok)
    operands = dict(
        latent=kv_latent[0], key=rope_key[0], lgain=latent_norm_gain[None],
        row_table=row_table, col_table=col_table, routes=routes[0].T,
        q=queries[0], kup=key_up_weight, vup=value_up_weight, res=residual[0],
        oproj=out_proj, gain=ffn_gain[None], weights=route_weights[0].T,
        gate=expert_gate[0], up=expert_up[0], down=expert_down[0],
    )
    fused = capacity % 16 == 0
    results = layer(operands, sp_size, dp_size, capacity, fused)
    if fused:
        normed, layer_out = results
        return (normed[None], layer_out[None])
    normed, mixed, outgoing, pick = results
    blocks = outgoing.reshape(experts, capacity, d)
    slot_rows = exchange(blocks, dp_size, 1).reshape(experts * capacity, d)
    expert_out = expert_rows(slot_rows, expert_gate[0], expert_up[0], expert_down[0])
    back = exchange(expert_out.reshape(blocks.shape), dp_size, 2)
    layer_out = combine(pick, back.reshape(experts * capacity, d), route_weights[0], mixed)
    return (normed[None], layer_out[None])


def solution(mesh):
    in_specs = (
        P("dp", "sp", None),
        P("dp", "sp", None),
        P("dp", "sp", None),
        P(),
        P(),
        P(),
        P(),
        P("dp", "sp", None),
        P(),
        P("dp", "sp", None),
        P("dp", "sp", None),
        P(("sp", "dp"), None, None),
        P(("sp", "dp"), None, None),
        P(("sp", "dp"), None, None),
    )
    out_specs = (P("dp", "sp", None), P("dp", "sp", None))
    return jax.shard_map(local, mesh=mesh, in_specs=in_specs, out_specs=out_specs, check_vma=False)
```

time: 187 us -> 134 us (0.72)
  the two profiles are of different devices: /device:TPU:15 before, /device:TPU:31 now
where the time goes in v2:
time: 134 us; the launch traced here: 133 us
  Pallas kernels  127 us (95%)
  local copies, waits for them, and re-layouts  5.18 us (4%)
    pallas_call x1, Pallas kernels, layer(): pl.pallas_call(functools.partial(layer_kernel, names, (sp_size, dp_size,...  127 us
    unnamed x3, local copies, waits for them, and re-layouts  5.18 us

profile of v2, /device:TPU:31, one launch (start us, length us, event | category | flops | bytes accessed | tf_op | source)
XLA Modules:
  0.0 133.3 jit_solution(9945107876140223139)
XLA Ops:
  0.6 1.4 %copy.18 = bf16[1,128,32]{2,1,0:T(8,128)(2,1)} copy(bf16[1,128,32]{1,2,0:T(8,128)(2,1)} %param.18) | data formatting | bytes 16384 | tf_op args[2]
  2.0 127.5 %layer.1 = (bf16[128,2048]{1,0:T(8,128)(2,1)}, bf16[128,2048]{1,0:T(8,128)(2,1)}) custom-call(bf16[128,256]{1,0:T(8,128)(2,1)} %bitcast.25, bf16[128,32]{1,0:T(8,128)(2,1)} %bitcast.24, f32[1,256]{1,0:T(1,128)} %bitcast.27, f32[32,1152]{1,0:T(8,128)} %constant.4.clone.refs_3_, f32[64,1152]{1,0:T(8,128)} %constant.5.clone.refs_4_, s32[2,128]{1,0:T(2,128)} %bitcast.28, ...), custom_call_target="tpu_custom_call" | custom-call | tf_op jit(solution)/shard_map/layer/pallas_call | solution.py:739
  129.5 1.9 %copy.21 = bf16[1,128,2048]{2,1,0:T(8,128)(2,1)} copy(bf16[1,128,2048]{2,1,0:T(8,128)(2,1)} %bitcast.23) | data formatting | bytes 1048576
  131.4 1.9 %copy.22 = bf16[1,128,2048]{2,1,0:T(8,128)(2,1)} copy(bf16[1,128,2048]{2,1,0:T(8,128)(2,1)} %bitcast.22) | data formatting | bytes 1048576

commit v3 on v2

--- a/solution.py
+++ b/solution.py
@@ -25,7 +25,7 @@
 BF16 = jnp.bfloat16
 MESH_ID = pl.DeviceIdType.MESH
 VMEM_LIMIT = 60 * 1024 * 1024
-LAYER_VMEM = 63 * 1024 * 1024 + 900 * 1024
+LAYER_VMEM = 61 * 1024 * 1024
 
 
 def params(**kw):
@@ -216,8 +216,8 @@
     blocks[sp, :tok, :] = latent.astype(BF16)
     key = r.key[...].astype(F32)
     key = jnp.concatenate(
-        [jnp.zeros((tok, PLAIN), F32), key, jnp.zeros((tok, 128 - QK), F32)], axis=1
-    )
+        [jnp.zeros((PLAIN, tok), F32), key, jnp.zeros((128 - QK, tok), F32)], axis=0
+    ).T
     key_columns = turn(key, 128).T.astype(BF16)
     blocks[sp, tok:, :tok] = key_columns[PLAIN : PLAIN + half_rot]
     blocks[sp, tok:, tok:] = key_columns[PLAIN + half_rot : QK]
@@ -538,7 +538,7 @@
 
         def answer(block, other):
             return remote(
-                r.outbox.at[block, other], r.back.at[me],
+                r.stage.at[block, other], r.back.at[me],
                 r.back_send.at[block * near + other], r.back_recv.at[me],
                 block * PLANE + other // dp_size, lax.rem(other, dp_size),
             )
@@ -559,6 +559,11 @@
                 return 0
 
             lax.fori_loop(1, near, wait, 0)
+            def given_out(k, _):
+                give(block, lax.rem(mine + k, near)).wait_send()
+                return 0
+
+            lax.fori_loop(1, near, given_out, 0)
             x = r.inbox[block].reshape(near * capacity, d)
             for n in range(0, r.gate.shape[1], 256):
                 at = slice(n, n + 256)
@@ -568,11 +573,11 @@
                 r.hidden[:, at] = hidden.astype(BF16)
             for n in range(0, d, tile):
                 part = dot(r.hidden[...], r.down[:, n : n + tile]).astype(BF16)
-                r.outbox[block, :, :, n : n + tile] = part.reshape(near, capacity, tile)
+                r.stage[block, :, :, n : n + tile] = part.reshape(near, capacity, tile)
 
             @pl.when(block == z)
             def _():
-                r.back[me] = r.outbox[block, mine]
+                r.back[me] = r.stage[block, mine]
 
             answer_all(block, start)
 
@@ -580,7 +585,8 @@
             loads[name].wait()
 
         def at_hop(t, act):
-            block = z + jnp.where(lax.rem(t, 2) == 1, -((t + 1) // 2), t // 2)
+            toward = jnp.where(z < line // 2, 1, -1)
+            block = z + toward * jnp.where(lax.rem(t, 2) == 1, (t + 1) // 2, -(t // 2))
 
             @pl.when((block >= 0) & (block < line))
             def _():
@@ -615,22 +621,36 @@
         pick_rows()
         weights = columns(r.weights[...])
 
-        def wait_back(k, _):
-            other = lax.rem(me + k, experts)
-            remote(
-                r.outbox.at[0, 0], r.back.at[other], r.back_send.at[0], r.back_recv.at[other], sp, dp
-            ).wait_recv()
+        def combine(block):
+            def wait_back(k, _):
+                other = block * near + k
+
+                @pl.when(other != me)
+                def _():
+                    remote(
+                        r.stage.at[0, 0], r.back.at[other],
+                        r.back_send.at[0], r.back_recv.at[other], sp, dp,
+                    ).wait_recv()
+
+                return 0
+
+            lax.fori_loop(0, near, wait_back, 0)
+            span = near * capacity
+            pick = r.pick[:, pl.ds(pl.multiple_of(block * span, 128), span)]
+            for n in range(0, d, tile):
+                back = r.back[pl.ds(block * near, near), :, n : n + tile]
+                picked = dot(pick, back.reshape(span, tile))
+                total = r.mixed[:, n : n + tile]
+                for k in range(topk):
+                    total = total + picked[k * tok : (k + 1) * tok] * weights[:, k : k + 1]
+                r.mixed[:, n : n + tile] = total
+
+        def combine_hop(t, _):
+            at_hop(t, combine)
             return 0
 
-        lax.fori_loop(1, experts, wait_back, 0)
-        for n in range(0, d, tile):
-            back = r.back[:, :, n : n + tile].reshape(experts * capacity, tile)
-            picked = dot(r.pick[...], back)
-            routed = None
-            for k in range(topk):
-                term = picked[k * tok : (k + 1) * tok] * weights[:, k : k + 1]
-                routed = term if routed is None else routed + term
-            r.out[:, n : n + tile] = (r.mixed[:, n : n + tile] + routed).astype(BF16)
+        lax.fori_loop(0, hops, combine_hop, 0)
+        r.out[...] = r.mixed[...].astype(BF16)
 
         def finish(block, _):
             def drain(c):
@@ -640,11 +660,6 @@
                 ship_both(block, h, drain)
             answer_all(block, drain)
 
-            def sent_all(k, _):
-                give(block, lax.rem(mine + k, near)).wait_send()
-                return 0
-
-            lax.fori_loop(1, near, sent_all, 0)
             return 0
 
         lax.fori_loop(0, line, finish, 0)
@@ -719,7 +734,6 @@
             tokens=vmem((line, tok, d), BF16),
             stage=vmem((line, near, capacity, d), BF16),
             inbox=vmem((line, near, capacity, d), BF16),
-            outbox=vmem((line, near, capacity, d), BF16),
             back=vmem((experts, capacity, d), BF16),
             hidden=vmem((near * capacity, ff), BF16),
             route_send=dma((line,)),
@@ -740,7 +754,7 @@
         functools.partial(layer_kernel, names, (sp_size, dp_size, experts, capacity, fused)),
         in_specs=[pl.BlockSpec(memory_space=pl.ANY)] * len(inputs),
         out_specs=[pl.BlockSpec(memory_space=pltpu.VMEM)] * len(outputs),
-        out_shape=list(outputs.values()),
+        out_shape=[pltpu.VMEM(o.shape, o.dtype) if fused else o for o in outputs.values()],
         scratch_shapes=list(scratch.values()),
         compiler_params=params(
             collective_id=0, has_side_effects=True, vmem_limit_bytes=LAYER_VMEM
@@ -847,13 +861,13 @@
     capacity = max(2, 2 * tok * topk // experts)
     row_table, col_table = turn_tables(sp_size * tok)
     operands = dict(
-        latent=kv_latent[0], key=rope_key[0], lgain=latent_norm_gain[None],
+        latent=kv_latent[0], key=rope_key[0].T, lgain=latent_norm_gain[None],
         row_table=row_table, col_table=col_table, routes=routes[0].T,
         q=queries[0], kup=key_up_weight, vup=value_up_weight, res=residual[0],
         oproj=out_proj, gain=ffn_gain[None], weights=route_weights[0].T,
         gate=expert_gate[0], up=expert_up[0], down=expert_down[0],
     )
-    fused = capacity % 16 == 0
+    fused = capacity % 16 == 0 and PLANE * dp_size * capacity % 128 == 0
     results = layer(operands, sp_size, dp_size, capacity, fused)
     if fused:
         normed, layer_out = results

time: 134 us -> 124 us (0.925)
  the two profiles are of different devices: /device:TPU:31 before, /device:TPU:15 now
where the time goes in v3:
time: 124 us; the launch traced here: 122 us
  Pallas kernels  120 us (97%)
  local copies, waits for them, and re-layouts  1.59 us (1%)
    pallas_call x1, Pallas kernels, layer(): pl.pallas_call(functools.partial(layer_kernel, names, (sp_size, dp_size,...  120 us

profile of v3, /device:TPU:15, one launch (start us, length us, event | category | flops | bytes accessed | tf_op | source)
XLA Modules:
  0.0 122.0 jit_solution(7369167600355205194)
XLA Ops:
  0.6 119.7 %layer.1 = (bf16[128,2048]{1,0:T(8,128)(2,1)S(1)}, bf16[128,2048]{1,0:T(8,128)(2,1)S(1)}) custom-call(bf16[128,256]{1,0:T(8,128)(2,1)} %bitcast.26, bf16[32,128]{1,0:T(8,128)(2,1)} %bitcast.27, f32[1,256]{1,0:T(1,128)} %bitcast.29, f32[32,1152]{1,0:T(8,128)} %constant.4.clone.refs_3_, f32[64,1152]{1,0:T(8,128)} %constant.5.clone.refs_4_, s32[2,128]{1,0:T(2,128)} %bitcast.30, ...), custom_call_target="tpu_custom_call" | custom-call | tf_op jit(solution)/shard_map/layer/pallas_call | solution.py:753
  120.4 0.8 copy.20
  121.2 0.8 copy.21

commit v4 on v3

--- a/solution.py
+++ b/solution.py
@@ -181,19 +181,19 @@
         greet(x_near, dp)
         greet(y_near, dp)
 
-    loaded = [
-        "latent", "key", "lgain", "row_table", "col_table", "routes",
-        "q", "kup", "vup", "res", "oproj", "gain",
-    ]
+    first = ["latent", "key", "lgain", "row_table", "col_table", "routes"]
     if fused:
-        loaded += ["weights", "gate", "up", "down"]
+        first.append("weights")
+    loaded = first + ["q", "kup", "vup", "res", "oproj", "gain"]
+    if fused:
+        loaded += ["gate", "up", "down"]
     loads = {
         name: pltpu.make_async_copy(getattr(r, name + "_hbm"), getattr(r, name), r.load_sem.at[i])
         for i, name in enumerate(loaded)
     }
     for name in loaded:
         loads[name].start()
-    for name in loaded[:6]:
+    for name in first:
         loads[name].wait()
 
     grid_rows = tok // GRID_W
@@ -223,7 +223,8 @@
     blocks[sp, tok:, tok:] = key_columns[PLAIN + half_rot : QK]
     if fused:
         r.line_routes[z] = jnp.concatenate(
-            [r.routes[...], jnp.zeros((8 - topk, tok), jnp.int32)], axis=0
+            [r.routes[...].astype(F32), r.weights[...], jnp.zeros((8 - 2 * topk, tok), F32)],
+            axis=0,
         )
 
     def remote(src, dst, send, recv, place, other_dp):
@@ -458,28 +459,29 @@
     step(2 * groups - 1, None, 0)
     settle(1)
 
-    expert_lane = lax.broadcasted_iota(jnp.int32, (tok, experts), 1)
-    slot_lane = lax.broadcasted_iota(jnp.int32, (tok, experts * capacity), 1)
     place_a = lax.broadcasted_iota(jnp.int32, (tok, tok), 0)
     place_b = lax.broadcasted_iota(jnp.int32, (tok, tok), 1)
 
+    earlier = (place_b < place_a).astype(BF16)
+
     def columns(part):
-        rest = jnp.zeros((tok - topk, tok), F32)
+        rest = jnp.zeros((tok - part.shape[0], tok), F32)
         return jnp.concatenate([part.astype(F32), rest], axis=0).T
 
-    def pick_rows():
-        routes = columns(r.routes[...])
-        earlier = (place_b < place_a).astype(BF16)
-        taken = jnp.zeros((1, experts), F32)
+    def pick_rows(routes, base, count, dest):
+        expert_lane = lax.broadcasted_iota(jnp.int32, (tok, count), 1)
+        slot_lane = lax.broadcasted_iota(jnp.int32, (tok, count * capacity), 1)
+        taken = jnp.zeros((1, count), F32)
         picks = []
         for k in range(topk):
-            expert = routes[:, k : k + 1].astype(jnp.int32)
+            expert = routes[:, k : k + 1].astype(jnp.int32) - base
             named = (expert_lane == expert).astype(F32)
             before = dot(earlier, named.astype(BF16)) + taken
             rank = jnp.sum(before * named, axis=1, keepdims=True)
-            slot = expert * capacity + rank.astype(jnp.int32)
+            mine = jnp.sum(named, axis=1, keepdims=True) > 0
+            slot = jnp.where(mine, expert * capacity + rank.astype(jnp.int32), -1)
             pick = (slot_lane == slot).astype(F32)
-            r.pick[k * tok : (k + 1) * tok, :] = pick.astype(BF16)
+            dest[k * tok : (k + 1) * tok, :] = pick.astype(BF16)
             picks.append(pick)
             taken = taken + jnp.sum(named, axis=0, keepdims=True)
         return picks
@@ -516,8 +518,8 @@
             taken = jnp.zeros((near, 1), F32)
             spread = None
             for k in range(topk):
-                route = r.line_routes[block, k : k + 1, :] - z * near
-                named = (local_row == route).astype(F32)
+                route = r.line_routes[block, k : k + 1, :] - (z * near).astype(F32)
+                named = (local_row.astype(F32) == route).astype(F32)
                 before = dot(named, later) + taken
                 slot = local_row.astype(F32) * capacity + before + 1.0
                 slot = jnp.sum(named * slot, axis=0, keepdims=True).astype(jnp.int32) - 1
@@ -543,11 +545,29 @@
                 block * PLANE + other // dp_size, lax.rem(other, dp_size),
             )
 
+        split = line // 2
+        low = z < split
+        gate_z = jnp.where(low, split - 1, split)
+        beyond = jnp.where(low, split, split - 1)
+        base = jnp.where(low, 0, split * near)
+        joint = split * near
+
+        def answer_gate(block, other):
+            return remote(
+                r.stage.at[block, other], r.gate_in.at[me - base],
+                r.back_send.at[block * near + other], r.gate_recv.at[me - base],
+                gate_z * PLANE + other // dp_size, lax.rem(other, dp_size),
+            )
+
         def answer_all(block, act):
             def one(other, _):
-                @pl.when((block != z) | (other != mine))
+                @pl.when((block != beyond) & ((block != z) | (other != mine)))
                 def _():
                     act(answer(block, other))
+
+                @pl.when((block == beyond) & ((gate_z != z) | (other != mine)))
+                def _():
+                    act(answer_gate(block, other))
 
                 return 0
 
@@ -579,9 +599,46 @@
             def _():
                 r.back[me] = r.stage[block, mine]
 
-            answer_all(block, start)
-
-        for name in ("weights", "gate", "up", "down"):
+            @pl.when((block == beyond) & (gate_z == z))
+            def _():
+                r.gate_in[me - base] = r.stage[block, mine]
+
+            @pl.when(((block < split) != low))
+            def _():
+                answer_all(block, start)
+
+        def joined(start_from):
+            return remote(
+                r.gate_out, r.joined, r.join_send, r.join_recv,
+                start_from * PLANE + p, dp,
+            )
+
+        def join():
+            theirs = columns(r.line_routes[beyond])
+            pick_rows(theirs, base, joint, r.gate_pick)
+
+            def wait_gate(k, _):
+                @pl.when(k != me - base)
+                def _():
+                    remote(
+                        r.stage.at[0, 0], r.gate_in.at[k],
+                        r.back_send.at[0], r.gate_recv.at[k], sp, dp,
+                    ).wait_recv()
+
+                return 0
+
+            lax.fori_loop(0, joint, wait_gate, 0)
+            for n in range(0, d, tile):
+                rows_in = r.gate_in[:, :, n : n + tile].reshape(joint * capacity, tile)
+                picked = dot(r.gate_pick[...], rows_in)
+                total = None
+                for k in range(topk):
+                    term = picked[k * tok : (k + 1) * tok] * theirs[:, topk + k : topk + k + 1]
+                    total = term if total is None else total + term
+                r.gate_out[:, n : n + tile] = total.astype(BF16)
+            joined(beyond).start()
+
+        for name in ("gate", "up", "down"):
             loads[name].wait()
 
         def at_hop(t, act):
@@ -618,8 +675,23 @@
             return 0
 
         lax.fori_loop(0, hops + lag, hop, 0)
-        pick_rows()
-        weights = columns(r.weights[...])
+
+        def answer_late(block, _):
+            @pl.when(jnp.logical_not(((block < split) != low)))
+            def _():
+                answer_all(block, start)
+
+            return 0
+
+        lax.fori_loop(0, line, answer_late, 0)
+        rows_of = columns(r.line_routes[z])
+        pick_rows(rows_of, 0, experts, r.pick)
+        weights = rows_of[:, topk : 2 * topk]
+
+        @pl.when(z == gate_z)
+        def _():
+            join()
+
 
         def combine(block):
             def wait_back(k, _):
@@ -646,10 +718,22 @@
                 r.mixed[:, n : n + tile] = total
 
         def combine_hop(t, _):
-            at_hop(t, combine)
+            def mine_only(block):
+                @pl.when((z != gate_z) | ((block < split) == low))
+                def _():
+                    combine(block)
+
+            at_hop(t, mine_only)
             return 0
 
         lax.fori_loop(0, hops, combine_hop, 0)
+
+        @pl.when(z == gate_z)
+        def _():
+            joined(beyond).wait_recv()
+            joined(beyond).wait_send()
+            r.mixed[...] = r.mixed[...] + r.joined[...].astype(F32)
+
         r.out[...] = r.mixed[...].astype(BF16)
 
         def finish(block, _):
@@ -664,7 +748,9 @@
 
         lax.fori_loop(0, line, finish, 0)
     else:
-        spread = functools.reduce(jnp.add, pick_rows()).T.astype(BF16)
+        spread = functools.reduce(
+            jnp.add, pick_rows(columns(r.routes[...]), 0, experts, r.pick)
+        ).T.astype(BF16)
         r.slots[...] = dot(spread, r.normed[...]).astype(BF16)
 
     def sent(k, _):
@@ -730,7 +816,7 @@
         scratch.update(
             mixed=vmem((tok, d), F32),
             pick=vmem((topk * tok, slots), BF16),
-            line_routes=vmem((line, 8, tok), jnp.int32),
+            line_routes=vmem((line, 8, tok), F32),
             tokens=vmem((line, tok, d), BF16),
             stage=vmem((line, near, capacity, d), BF16),
             inbox=vmem((line, near, capacity, d), BF16),
@@ -744,6 +830,13 @@
             give_recv=dma((line * near,)),
             back_send=dma((line * near,)),
             back_recv=dma((experts,)),
+            gate_in=vmem((line // 2 * near, capacity, d), BF16),
+            gate_out=vmem((tok, d), BF16),
+            gate_pick=vmem((topk * tok, line // 2 * near * capacity), BF16),
+            joined=vmem((tok, d), BF16),
+            gate_recv=dma((line // 2 * near,)),
+            join_send=dma,
+            join_recv=dma,
         )
     else:
         outputs["mixed"] = jax.ShapeDtypeStruct((tok, d), F32)
@@ -868,6 +961,7 @@
         gate=expert_gate[0], up=expert_up[0], down=expert_down[0],
     )
     fused = capacity % 16 == 0 and PLANE * dp_size * capacity % 128 == 0
+    fused = fused and sp_size % (2 * PLANE) == 0
     results = layer(operands, sp_size, dp_size, capacity, fused)
     if fused:
         normed, layer_out = results

time: 124 us -> 117 us (0.944)
  Pallas kernels: 120 us -> 113 us
    pallas_call x1, Pallas kernels: 120 us -> 113 us  [layer(): pl.pallas_call(functools.partial(layer_kernel, names, (sp_size, dp_size,...]
where the time goes in v4:
time: 117 us; the launch traced here: 115 us
  Pallas kernels  113 us (97%)
  local copies, waits for them, and re-layouts  1.59 us (1%)
    pallas_call x1, Pallas kernels, layer(): pl.pallas_call(functools.partial(layer_kernel, names, (sp_size, dp_size,...  113 us

profile of v4, /device:TPU:15, one launch (start us, length us, event | category | flops | bytes accessed | tf_op | source)
XLA Modules:
  0.0 115.3 jit_solution(9046049975862640875)
XLA Ops:
  0.6 113.1 %layer.1 = (bf16[128,2048]{1,0:T(8,128)(2,1)S(1)}, bf16[128,2048]{1,0:T(8,128)(2,1)S(1)}) custom-call(bf16[128,256]{1,0:T(8,128)(2,1)} %bitcast.26, bf16[32,128]{1,0:T(8,128)(2,1)} %bitcast.27, f32[1,256]{1,0:T(1,128)} %bitcast.29, f32[32,1152]{1,0:T(8,128)} %constant.4.clone.refs_3_, f32[64,1152]{1,0:T(8,128)} %constant.5.clone.refs_4_, s32[2,128]{1,0:T(2,128)} %bitcast.30, ...), custom_call_target="tpu_custom_call" | custom-call | tf_op jit(solution)/shard_map/layer/pallas_call | solution.py:846
  113.7 0.8 copy.20
  114.5 0.8 copy.21

commit v5 on v4

--- a/solution.py
+++ b/solution.py
@@ -560,7 +560,9 @@
             )
 
         def answer_all(block, act):
-            def one(other, _):
+            def one(k, _):
+                other = lax.rem(mine + k, near)
+
                 @pl.when((block != beyond) & ((block != z) | (other != mine)))
                 def _():
                     act(answer(block, other))
@@ -658,15 +660,16 @@
                 def _():
                     forward(block, 0)
 
-                @pl.when(t > 0)
-                def _():
-                    forward(block, 1)
-
-                dispatch(block)
+                forward(block, 1)
+
+            @pl.when((t < hops) & (lax.rem(t, 2) == 1))
+            def _():
+                at_hop(t + 1, bring)
+                at_hop(t, bring)
 
             @pl.when(t < hops)
             def _():
-                at_hop(t, bring)
+                at_hop(t, dispatch)
 
             @pl.when(t >= lag)
             def _():

time: 117 us -> 116 us (level)
  Pallas kernels: 113 us -> 111 us
    pallas_call x1, Pallas kernels: 113 us -> 111 us  [layer(): pl.pallas_call(functools.partial(layer_kernel, names, (sp_size, dp_size,...]
where the time goes in v5:
time: 116 us; the launch traced here: 114 us
  Pallas kernels  111 us (96%)
  local copies, waits for them, and re-layouts  1.59 us (1%)
    pallas_call x1, Pallas kernels, layer(): pl.pallas_call(functools.partial(layer_kernel, names, (sp_size, dp_size,...  111 us

profile of v5, /device:TPU:15, one launch (start us, length us, event | category | flops | bytes accessed | tf_op | source)
XLA Modules:
  0.0 113.5 jit_solution(17197423893212442519)
XLA Ops:
  0.6 111.3 %layer.1 = (bf16[128,2048]{1,0:T(8,128)(2,1)S(1)}, bf16[128,2048]{1,0:T(8,128)(2,1)S(1)}) custom-call(bf16[128,256]{1,0:T(8,128)(2,1)} %bitcast.26, bf16[32,128]{1,0:T(8,128)(2,1)} %bitcast.27, f32[1,256]{1,0:T(1,128)} %bitcast.29, f32[32,1152]{1,0:T(8,128)} %constant.4.clone.refs_3_, f32[64,1152]{1,0:T(8,128)} %constant.5.clone.refs_4_, s32[2,128]{1,0:T(2,128)} %bitcast.30, ...), custom_call_target="tpu_custom_call" | custom-call | tf_op jit(solution)/shard_map/layer/pallas_call | solution.py:849
  111.9 0.8 copy.20
  112.7 0.8 copy.21
